TPU v7x, 256 devices: a whole 4x4x8 slice. The times are simulated.
256 devices in a mesh: rep: 2 (over z_hi), fs: 16 (over z_lo, x), tp: 8 (over y, core).
Axes of the slice: x: 4, y: 4, z: 8 (z_hi: 2, z_lo: 4; z = z_hi * 4 + z_lo), core: 2. Of those that a mesh axis runs over, the one named last changes fastest.
Arguments:
- tokens: bfloat16 [32768, 2048], P(('rep', 'fs'), 'tp'), may hold values from -6 to 6
- mix_gain: float32 [2048], replicated, may hold values from 0.1 to 1.9
- query_weight: bfloat16 [2048, 512], P('fs', 'tp'), may hold values from -0.125 to 0.125
- key_weight: bfloat16 [2048, 512], P('fs', 'tp'), may hold values from -0.125 to 0.125
- value_weight: bfloat16 [2048, 1024], P('fs', 'tp'), may hold values from -0.125 to 0.125
- gate_weight: bfloat16 [2048, 1024], P('fs', 'tp'), may hold values from -0.125 to 0.125
- out_weight: bfloat16 [1024, 2048], P('tp', 'fs'), may hold values from -0.1875 to 0.1875
- head_gain: float32 [8, 128], P('tp'), may hold values from 0.1 to 1.9
- ffn_gain: float32 [2048], replicated, may hold values from 0.1 to 1.9
- ffn_gate: bfloat16 [2048, 5632], P('fs', 'tp'), may hold values from -0.125 to 0.125
- ffn_up: bfloat16 [2048, 5632], P('fs', 'tp'), may hold values from -0.125 to 0.125
- ffn_down: bfloat16 [5632, 2048], P('tp', 'fs'), may hold values from -0.078125 to 0.078125
Outputs:
- layer_out: bfloat16 [32768, 2048], P(('rep', 'fs'), 'tp')
All inputs are finite; a program needn't handle non-finite values.
Results may differ from a plain program's by a relative error of at most 0.03.
Values may be sent and summed in bfloat16 or wider, within the bound.
A program may use at most 128 MiB of HBM per device.

v0:
```python
import jax
import jax.numpy as jnp
from jax import lax
from jax.sharding import Mesh
from jax.sharding import PartitionSpec as P

HEADS = 8
DK = 64
DV = 128
BLOCK = 64
SEQ = 256
FS = ("fs_0", "fs_1")
REP_FS = ("rep", "fs_0", "fs_1")


epsilon = 1e-06
rope_base = 10000.0


def in_one_piece(arrays, axis, dim, along):
    widths = [a.shape[along] for a in arrays]
    both = jnp.concatenate(arrays, axis=along)
    out = lax.all_gather(both, axis, axis=dim, tiled=True)
    return tuple(jnp.split(out, [sum(widths[:k]) for k in range(1, len(widths))], axis=along))


def joined_along(pieces, dim):
    shape = list(pieces.shape[1:])
    shape[dim] *= pieces.shape[0]
    return jnp.moveaxis(pieces, 0, dim).reshape(shape)


def sent_to_all(array, axis):
    size = lax.axis_size(axis)
    return lax.all_to_all(
        jnp.broadcast_to(array[None], (size, *array.shape)), axis, 0, 0, tiled=True
    )


def collect(array, axis, dim):
    return joined_along(sent_to_all(array, axis), dim)


def cut_along(array, dim, size):
    shape = array.shape
    pieces = array.reshape(*shape[:dim], size, shape[dim] // size, *shape[dim + 1 :])
    return jnp.moveaxis(pieces, dim, 0)


def sent_and_summed(array, axis, dim):
    size = lax.axis_size(axis)
    pieces = lax.all_to_all(cut_along(array, dim, size), axis, 0, 0, tiled=True)
    return jnp.sum(pieces.astype(jnp.float32), axis=0)


def gather_in_order(array, axes, order):
    pieces = array[None]
    for k in order:
        pieces = lax.all_gather(pieces, axes[k], axis=0, tiled=True)
    block = [lax.axis_size(axes[k]) for k in reversed(order)]
    pieces = pieces.reshape(*block, *array.shape)
    turned = sorted(range(len(order)), key=lambda place: order[len(order) - 1 - place])
    return pieces.transpose(*turned, *range(len(order), pieces.ndim)).reshape(-1, *array.shape)


def gathered_by_axis(array, axes, order, dim):
    return joined_along(gather_in_order(array, axes, order), dim)


def norm_rows(values, gain_row):
    floats = values.astype(jnp.float32)
    scaled = floats * lax.rsqrt(jnp.mean(floats * floats, axis=-1, keepdims=True) + epsilon)
    return (scaled * gain_row).astype(jnp.bfloat16)


def rotate(values, positions):
    half_dim = values.shape[-1] // 2
    frequency = rope_base ** (-jnp.linspace(0.0, 1.0, half_dim, dtype=jnp.float32))
    angles = positions.astype(jnp.float32)[:, None] * frequency[None, :]
    cosine = jnp.cos(angles)[:, None, :]
    sine_part = jnp.sin(angles)[:, None, :]
    paired = values.reshape(values.shape[:-1] + (half_dim, 2))
    leading = paired[..., 0]
    trailing = paired[..., 1]
    turned = jnp.stack(
        [leading * cosine - trailing * sine_part, leading * sine_part + trailing * cosine], axis=-1
    )
    return turned.reshape(values.shape)


def log_decay(head_index, total_heads):
    return jnp.log1p(-jnp.exp2(-5.0 - 4.0 * head_index.astype(jnp.float32) / (total_heads - 1)))


def retention(queries, key_rows, value_rows, decay_rates):
    highest = lax.Precision.HIGHEST
    row_count, head_count = (queries.shape[0], queries.shape[1])
    seq_count = row_count // SEQ
    block_count = SEQ // BLOCK

    def to_blocks(values):
        shaped = values.reshape((seq_count, block_count, BLOCK) + values.shape[1:])
        return jnp.moveaxis(shaped, 1, 0)

    inside = jnp.arange(BLOCK, dtype=jnp.int32)
    gap = (inside[:, None] - inside[None, :]).astype(jnp.float32)
    within_mask = jnp.where(
        gap[None] >= 0.0, jnp.exp(jnp.maximum(gap, 0.0)[None] * decay_rates[:, None, None]), 0.0
    )
    query_scale = jnp.exp((inside + 1).astype(jnp.float32)[:, None] * decay_rates[None, :])
    key_scale = jnp.exp((BLOCK - 1 - inside).astype(jnp.float32)[:, None] * decay_rates[None, :])
    block_decay = jnp.exp(BLOCK * decay_rates)

    def advance(state, inputs):
        query_blk, key_blk, value_blk = inputs
        scores = (
            jnp.einsum("sihd,sjhd->shij", query_blk, key_blk, precision=highest) * within_mask[None]
        )
        local_part = jnp.einsum("shij,sjhv->sihv", scores, value_blk, precision=highest)
        carried = jnp.einsum(
            "sihd,shdv->sihv", query_blk * query_scale[None, :, :, None], state, precision=highest
        )
        update = jnp.einsum(
            "sjhd,sjhv->shdv", key_blk * key_scale[None, :, :, None], value_blk, precision=highest
        )
        return (block_decay[None, :, None, None] * state + update, local_part + carried)

    state_zero = jnp.zeros((seq_count, head_count, DK, DV), jnp.float32)
    _, outputs = lax.scan(
        advance, state_zero, (to_blocks(queries), to_blocks(key_rows), to_blocks(value_rows))
    )
    return jnp.moveaxis(outputs, 0, 1).reshape(row_count, head_count, DV)


def per_device(
    tokens,
    mix_gain,
    query_weight,
    key_weight,
    value_weight,
    gate_weight,
    out_weight,
    head_gain,
    ffn_gain,
    ffn_gate,
    ffn_up,
    ffn_down,
):
    whole_rows = lax.all_gather(tokens, "tp", axis=1, tiled=True)
    row_count = whole_rows.shape[0]
    normed = norm_rows(whole_rows, mix_gain)
    pieces = in_one_piece((query_weight, key_weight, value_weight, gate_weight), FS, 0, 1)
    query_acc, key_acc, value_acc, gate_acc = tuple(
        (
            jnp.dot(normed, weight_piece, preferred_element_type=jnp.float32)
            for weight_piece in pieces
        )
    )
    heads_here = query_weight.shape[1] // DK
    positions = jnp.arange(row_count, dtype=jnp.int32) % SEQ
    queries = rotate(
        query_acc.astype(jnp.bfloat16).astype(jnp.float32).reshape(row_count, heads_here, DK),
        positions,
    )
    key_rows = rotate(
        key_acc.astype(jnp.bfloat16).astype(jnp.float32).reshape(row_count, heads_here, DK),
        positions,
    ) * DK ** (-0.5)
    value_rows = (
        value_acc.astype(jnp.bfloat16).astype(jnp.float32).reshape(row_count, heads_here, DV)
    )
    gate_rows = gate_acc.astype(jnp.bfloat16).astype(jnp.float32)
    first_head = lax.axis_index("tp") * heads_here
    decay_rates = log_decay(first_head + jnp.arange(heads_here, dtype=jnp.int32), HEADS)
    retained = retention(queries, key_rows, value_rows, decay_rates)
    center = jnp.mean(retained, axis=-1, keepdims=True)
    spread = jnp.mean(jnp.square(retained - center), axis=-1, keepdims=True)
    grouped = (retained - center) * lax.rsqrt(spread + epsilon) * head_gain[None]
    mixed = (grouped.reshape(row_count, heads_here * DV) * jax.nn.silu(gate_rows)).astype(
        jnp.bfloat16
    )
    mixer_terms = jnp.dot(mixed, collect(out_weight, FS, 1), preferred_element_type=jnp.float32)
    mixer_share = sent_and_summed(mixer_terms.astype(jnp.bfloat16), "tp", 1)
    resid_shard = (tokens.astype(jnp.float32) + mixer_share).astype(jnp.bfloat16)
    resid_whole = lax.all_gather(resid_shard, "tp", axis=1, tiled=True)
    normed_ffn = norm_rows(resid_whole, ffn_gain)

    def add_rows(weight_piece):
        return jnp.dot(normed_ffn, weight_piece, preferred_element_type=jnp.float32)

    gate_hidden = add_rows(gathered_by_axis(ffn_gate, FS, (0, 1), 0))
    up_hidden = add_rows(gathered_by_axis(ffn_up, FS, (0, 1), 0))
    hidden = (jax.nn.silu(gate_hidden) * up_hidden).astype(jnp.bfloat16)
    ffn_terms = jnp.dot(
        hidden, gathered_by_axis(ffn_down, FS, (0, 1), 1), preferred_element_type=jnp.float32
    )
    ffn_share = sent_and_summed(ffn_terms.astype(jnp.bfloat16), "tp", 1)
    return (resid_shard.astype(jnp.float32) + ffn_share).astype(jnp.bfloat16)


def solution(mesh):
    finer = Mesh(
        mesh.devices.reshape(mesh.shape["rep"], 4, 4, mesh.shape["tp"]),
        ("rep", "fs_0", "fs_1", "tp"),
    )
    placed = (
        P(REP_FS, "tp"),
        P(),
        P(FS, "tp"),
        P(FS, "tp"),
        P(FS, "tp"),
        P(FS, "tp"),
        P("tp", FS),
        P("tp", None),
        P(),
        P(FS, "tp"),
        P(FS, "tp"),
        P("tp", FS),
    )
    return jax.shard_map(
        per_device, mesh=finer, in_specs=placed, out_specs=P(REP_FS, "tp"), check_vma=False
    )
```

profile of v0, /device:TPU:1, one launch (start us, length us, event | category | flops | bytes accessed | tf_op | source)
XLA Modules:
  0.0 384.1 jit_solution(14955512853964494112)
XLA Ops:
  10.6 17.8 %all-gather = bf16[512,704]{0,1:T(8,128)(2,1)S(1)} all-gather(bf16[128,704]{0,1:T(8,128)(2,1)} %param.25), channel_id=2, replica_groups=mesh['rep'=2,'fs_0'=4,'fs_1'=4,'tp'=8] {'fs_0'}, dimensions={0}, use_global_device_ids=true | all-gather | bytes 901120 | tf_op jit(solution)/shard_map/all_gather | solution.py:59
  29.4 16.0 %all-gather.1 = bf16[512,704]{0,1:T(8,128)(2,1)S(1)} all-gather(bf16[128,704]{0,1:T(8,128)(2,1)} %param.26), channel_id=3, replica_groups=mesh['rep'=2,'fs_0'=4,'fs_1'=4,'tp'=8] {'fs_0'}, dimensions={0}, use_global_device_ids=true | all-gather | bytes 901120 | tf_op jit(solution)/shard_map/all_gather | solution.py:59
  47.5 4.2 %all-to-all-start = ((bf16[16,128,128]{1,2,0:T(8,128)(2,1)}), bf16[16,128,128]{1,2,0:T(8,128)(2,1)S(1)}, u32[]{:S(2)}, u32[]{:S(2)}) async-start(bf16[16,128,128]{1,2,0:T(8,128)(2,1)} %broadcast_in_dim.19), calls=%async_computation | async-start | bytes 1048576 | tf_op jit(solution)/shard_map/all_to_all | solution.py:35
  51.8 24.5 %all-gather.2 = bf16[2816,128]{1,0:T(8,128)(2,1)} all-gather(bf16[704,128]{1,0:T(8,128)(2,1)S(1)} %copy-done.6), channel_id=4, replica_groups=mesh['rep'=2,'fs_0'=4,'fs_1'=4,'tp'=8] {'fs_0'}, dimensions={0}, use_global_device_ids=true | all-gather | bytes 901120 | tf_op jit(solution)/shard_map/all_gather | solution.py:59
  76.7 3.2 fusion.26
  80.1 3.0 fusion.28
  83.1 43.1 %all-gather.12.cloned.1.call-done = bf16[2048,384]{1,0:T(8,128)(2,1)} async-done(((bf16[128,384]{1,0:T(8,128)(2,1)}), bf16[2048,384]{1,0:T(8,128)(2,1)}) %all-gather.12.cloned.1.call-update) | async-done | bytes 1572880 | tf_op jit(solution)/shard_map/all_gather | solution.py:23
  126.2 3.7 fusion.40
  130.3 3.7 convolution_convert_fusion.3
  134.0 2.5 fusion.41
  138.9 8.2 %while.15 = (s32[]{:T(128)}, f32[4,1,64,128]{3,2,0,1:T(8,128)S(1)}, f32[4,4,64,1,128]{4,2,1,3,0:T(8,128)S(1)}, f32[1]{0:T(128)}, f32[4,4,64,1,64]{2,0,1,4,3:T(4,...) while((s32[]{:T(128)}, f32[4,1,64,128]{3,2,0,1:T(8,128)S(1)}, ...), condition=%wide.region_2.4_spmd.clone.clone.clone, body=%wide.region_1.3_spmd.clone.clone.clone.sunk | while | flops 88318336 | bytes 2197140 | solution.py:129
  148.0 3.9 %fusion.49 = bf16[1024,128]{1,0:T(8,128)(2,1)S(1)} fusion(f32[4,4,64,1,128]{4,2,1,0,3:T(8,128)S(1)} %copy.104, bf16[1024,2048]{1,0:T(8,128)(2,1)} %fusion.28, bf16[2048,384]{1,0:T(8,128)(2,1)} %all-gather.12.cloned.1.call-done, f32[128]{0:T(128)S(1)} %bitcast.174, f32[1024]{0:T(1024)S(1)} %rsqrt.29, f32[1024]{0:T(1024)S(1)} %div.31), kind=kOutput, calls=%fused_computation.73 | convolution fusion | flops 538312704 | bytes 5513728 | tf_op jit(solution)/shard_map/dot_general | solution.py:155
  153.4 63.1 %all_to_all.15 = bf16[8,1024,256]{2,1,0:T(8,128)(2,1)S(1)} all-to-all(bf16[8,1024,256]{2,1,0:T(8,128)(2,1)S(1)} %bitcast.161), channel_id=1, replica_groups=mesh['rep'=2,'fs_0'=4,'fs_1'=4,'tp'=8] {'tp'}, dimensions={0} | all-to-all | bytes 8388608 | tf_op jit(solution)/shard_map/all_to_all | solution.py:52
  218.5 4.0 %copy.110 = bf16[4,4,128,704]{2,1,0,3:T(4,128)(2,1)S(1)} copy(bf16[4,4,128,704]{2,3,0,1:T(8,128)(2,1)} %bitcast.165) | data formatting | bytes 5767168 | tf_op jit(solution)/shard_map/transpose | solution.py:63
  222.6 3.4 reshape_reshape.31
  226.0 4.0 %copy.112 = bf16[4,4,128,704]{2,1,0,3:T(4,128)(2,1)S(1)} copy(bf16[4,4,128,704]{2,3,0,1:T(8,128)(2,1)} %bitcast.166) | data formatting | bytes 5767168 | tf_op jit(solution)/shard_map/transpose | solution.py:63
  230.0 3.4 reshape_reshape.32
  233.5 25.5 %all-gather.20.cloned.1.call-done = bf16[16,704,128]{2,1,0:T(8,128)(2,1)} async-done(((bf16[4,704,128]{2,1,0:T(8,128)(2,1)}), bf16[16,704,128]{2,1,0:T(8,128)(2,1)}) %all-gather.20.cloned.1.call-update) | async-done | bytes 2883600 | tf_op jit(solution)/shard_map/all_gather | solution.py:59
  259.0 3.8 copy.113
  262.9 36.7 %all-gather.14.cloned.1.call-done = bf16[1024,2048]{1,0:T(8,128)(2,1)} async-done(((bf16[1024,256]{1,0:T(8,128)(2,1)}), bf16[1024,2048]{1,0:T(8,128)(2,1)}) %all-gather.14.cloned.1.call-update) | async-done | bytes 4194320 | tf_op jit(solution)/shard_map/all_gather | solution.py:185
  299.6 3.2 fusion.29
  303.0 4.8 %fusion.35 = f32[1024,704]{0,1:T(8,128)} fusion(bf16[2048,704]{0,1:T(8,128)(2,1)S(1)} %copy-done.4, bf16[1024,2048]{1,0:T(8,128)(2,1)S(1)} %copy-done.3, f32[2048]{0:T(1024)S(1)} %copy-done.9, f32[1024]{0:T(1024)S(1)} %add_rsqrt_fusion.1), kind=kOutput, calls=%fused_computation.53 | convolution fusion | flops 2961178624 | bytes 9973760 | tf_op jit(solution)/shard_map/dot_general | solution.py:189
  307.8 12.4 %convolution_convert_fusion = bf16[1024,2048]{1,0:T(8,128)(2,1)} fusion(bf16[16,88,8,128]{3,2,1,0:T(8,128)(2,1)} %bitcast.168, f32[1024,704]{0,1:T(8,128)} %fusion.35, bf16[2048,704]{0,1:T(8,128)(2,1)} %reshape_reshape.32, bf16[1024,2048]{1,0:T(8,128)(2,1)} %all-gather.14.cloned.1.call-done, f32[2048]{0:T(1024)S(1)} %copy-done.9, f32[1024]{0:T(1024)S(1)} %add_rsqrt_fusion.1), kind=kOutput, calls=%fused_computation.48 | convolution fusion | flops 5920391168 | bytes 17051648 | tf_op jit(solution)/shard_map/dot_general | solution.py:194
  322.7 52.6 %all_to_all.16 = bf16[8,1024,256]{2,1,0:T(8,128)(2,1)S(1)} all-to-all(bf16[8,1024,256]{2,1,0:T(8,128)(2,1)S(1)} %bitcast.162), channel_id=1, replica_groups=mesh['rep'=2,'fs_0'=4,'fs_1'=4,'tp'=8] {'tp'}, dimensions={0} | all-to-all | bytes 8388608 | tf_op jit(solution)/shard_map/all_to_all | solution.py:52
  (115 shorter events, 26.9 us)
Async XLA Ops:
  6.5 40.0 %copy-start.7 = (bf16[128,128]{1,0:T(8,128)(2,1)S(1)}, bf16[128,128]{1,0:T(8,128)(2,1)}, u32[]{:S(2)}) copy-start(bf16[128,128]{1,0:T(8,128)(2,1)} %param.22) | copy-start | bytes 98308
  6.5 70.1 %all-gather.10.cloned.1.call-start = ((), (), s32[]{:S(2)}) async-start(), calls=%async_computation.3 | async-start | bytes 4718592 | tf_op jit(solution)/shard_map/all_gather | solution.py:149
  7.3 44.5 %copy-start.6 = (bf16[704,128]{1,0:T(8,128)(2,1)S(1)}, bf16[704,128]{1,0:T(8,128)(2,1)}, u32[]{:S(2)}) copy-start(bf16[704,128]{1,0:T(8,128)(2,1)} %param.27) | copy-start | bytes 540676
  7.3 118.9 %all-gather.12.cloned.1.call-start = ((), (), s32[]{:S(2)}) async-start(), calls=%async_computation.4 | async-start | bytes 1671168 | tf_op jit(solution)/shard_map/all_gather | solution.py:23
  10.5 208.0 %all-gather.16.cloned.1.call-start = ((), (), s32[]{:S(2)}) async-start(), calls=%async_computation.6 | async-start | bytes 3604480 | tf_op jit(solution)/shard_map/all_gather | solution.py:59
  29.4 196.6 %all-gather.18.cloned.1.call-start = ((), (), s32[]{:S(2)}) async-start(), calls=%async_computation.7 | async-start | bytes 3604480 | tf_op jit(solution)/shard_map/all_gather | solution.py:59
  46.5 33.4 %copy-start.8 = (f32[2048]{0:T(1024)S(1)}, f32[2048]{0:T(1024)}, u32[]{:S(2)}) copy-start(f32[2048]{0:T(1024)} %param.17) | copy-start | bytes 24580
  47.5 104.3 %all-to-all-start = ((bf16[16,128,128]{1,2,0:T(8,128)(2,1)}), bf16[16,128,128]{1,2,0:T(8,128)(2,1)S(1)}, u32[]{:S(2)}, u32[]{:S(2)}) async-start(bf16[16,128,128]{1,2,0:T(8,128)(2,1)} %broadcast_in_dim.19), calls=%async_computation | async-start | bytes 1048576 | tf_op jit(solution)/shard_map/all_to_all | solution.py:35
  51.7 207.3 %all-gather.20.cloned.1.call-start = ((), (), s32[]{:S(2)}) async-start(), calls=%async_computation.8 | async-start | bytes 3604480 | tf_op jit(solution)/shard_map/all_gather | solution.py:59
  76.3 223.2 %all-gather.14.cloned.1.call-start = ((), (), s32[]{:S(2)}) async-start(), calls=%async_computation.5 | async-start | bytes 4718592 | tf_op jit(solution)/shard_map/all_gather | solution.py:185
  76.7 3.5 copy-start.1
  130.1 4.0 %copy-start = (bf16[1024,2048]{1,0:T(8,128)(2,1)S(1)}, bf16[1024,2048]{1,0:T(8,128)(2,1)}, u32[]{:S(2)}) copy-start(bf16[1024,2048]{1,0:T(8,128)(2,1)} %fusion.28) | copy-start | bytes 12582916
  138.9 9.1 %copy-start.10 = (f32[1,128]{1,0:T(1,128)S(1)}, f32[1,128]{1,0:T(1,128)}, u32[]{:S(2)}) copy-start(f32[1,128]{1,0:T(1,128)} %param.23) | copy-start | bytes 1540
  216.5 1.0 copy-start.5
  259.0 43.8 %copy-start.4 = (bf16[2048,704]{0,1:T(8,128)(2,1)S(1)}, bf16[2048,704]{0,1:T(8,128)(2,1)}, u32[]{:S(2)}) copy-start(bf16[2048,704]{0,1:T(8,128)(2,1)} %reshape_reshape.31) | copy-start | bytes 8650756
  259.0 43.8 %copy-start.9 = (f32[2048]{0:T(1024)S(1)}, f32[2048]{0:T(1024)}, u32[]{:S(2)}) copy-start(f32[2048]{0:T(1024)} %param.24) | copy-start | bytes 24580
  299.6 3.4 copy-start.3
  375.3 1.0 copy-start.2
Sparse Core Ops, SparseCore 0:
  9.2 42.2 all-gather.9
  53.3 72.8 all-gather.11
  128.0 47.4 all-gather.15
  177.2 40.0 all-gather.17
  219.0 40.0 all-gather.19
  260.7 38.8 all-gather.13
where the time goes:
time: 385 us; the launch traced here: 384 us
  blocking collectives  174 us (45%)
  waiting for transfers between devices  106 us (28%)
  matrix products  37.9 us (10%)
  local copies, waits for them, and re-layouts  31.7 us (8%)
  other arithmetic  15.5 us (4%)
  between operations  13.9 us (4%)
  starting transfers between devices  4.38 us (1%)
    all_to_all x2, blocking collectives, sent_and_summed(): pieces = lax.all_to_all(cut_along(array, dim, size), axis, 0, 0, tiled=True)  116 us
    all_gather x3, blocking collectives, gather_in_order(): pieces = lax.all_gather(pieces, axes[k], axis=0, tiled=True)  58.3 us
    all_gather x1, waiting for transfers between devices, in_one_piece(): out = lax.all_gather(both, axis, axis=dim, tiled=True)  43.1 us
    all_gather x1, waiting for transfers between devices, per_device(): resid_whole = lax.all_gather(resid_shard, 'tp', axis=1, tiled=True)  36.7 us
    all_gather x3, waiting for transfers between devices, gather_in_order(): pieces = lax.all_gather(pieces, axes[k], axis=0, tiled=True)  25.6 us
    dot_general x4, matrix products, per_device(): jnp.dot(normed, weight_piece, preferred_element_type=jnp.float32)  13.8 us
    dot_general x1, matrix products, per_device(): jnp.dot(hidden, gathered_by_axis(ffn_down, FS, (0, 1), 1), preferred_elem...  12.4 us
    transpose x3, local copies, waits for them, and re-layouts, gather_in_order(): pieces.transpose(*turned, *range(len(order), pieces.ndim))  11.9 us
  transfers between devices with their start and end apart: 7, of which 3 were waited for; matrix products, arithmetic and copies ran while one was open for 15% of the time, Pallas kernels for 0%

commit v1 on v0

v1 whole, which is shorter than its diff:
```python
import functools

import jax
import jax.numpy as jnp
import numpy as np
from jax import lax
from jax.experimental import pallas as pl
from jax.experimental.pallas import tpu as pltpu
from jax.sharding import PartitionSpec as P

HEADS = 8
DK = 64
DV = 128
SEQ = 256
EPS = 1e-06
ROPE_BASE = 10000.0
F32 = jnp.float32
BF16 = jnp.bfloat16
MESH = pl.DeviceIdType.MESH
MAX_COPIES = 352

UNITS = {
    "QO": (0, 64, 32, 64, 32),
    "G0": (0, 32, 16, 32, 16),
    "G1": (64, 32, 16, 32, 16),
    "D0": (0, 176, 96, 176, 96),
    "D1": (352, 176, 96, 176, 96),
}

SCHEDULE = (
    "oz.QO", "ox.QO", "Tp.0", "stage_gu.0", "Tp.3", "g0z.QO", "ox.G0", "oz.G1",
    "g0x.QO", "fzp.QO", "fzm.QO", "fxp.QO", "fxm.QO", "Tp.2", "g1z.QO", "g2z.QO",
    "g2x.QO", "Tfa.0", "Tfb.0", "h0zp.QO", "g1x.QO", "h0xm.QO", "h0xp.QO", "h0zm.QO",
    "g3x.QO", "g3z.QO", "Tfb.3", "Tfa.3", "ox.G1", "oz.G0", "h2xm.QO", "Tp.1",
    "stage_c.0", "h1xp.QO", "h2xp.QO", "h1xm.QO", "h1zm.QO", "Tfb.2", "h1zp.QO", "h2zp.QO",
    "Tg.0", "h2zm.QO", "h3xp.QO", "h3xm.QO", "h3zp.QO", "h3zm.QO", "g0z.G0", "g0x.G0",
    "Tfa.2", "Tg.3", "Td.0", "fzm.G1", "norm1.0", "fzp.G1", "fzm.G0", "fxp.G0",
    "fzp.G0", "g1x.G0", "g1z.G0", "fxm.G0", "Td.3", "g2x.G0", "fxm.G1", "g0x.G1",
    "g2z.G0", "norm1.3", "stage_d.0", "oz.D0", "Tfa.1", "Tfb.1", "ox.D1", "oz.D1",
    "e.QO", "mixa.3", "Tg.2", "mixb.3", "Rx.3", "mixa.0", "mixb.0", "Rx.0",
    "Ra.3", "Td.2", "g3z.G0", "h0zp.G0", "g3x.G0", "fxp.G1", "g2z.G1", "h1zm.G0",
    "h0xp.G0", "h1xp.G0", "h0xm.G0", "Tg.1", "h0zm.G0", "h2xm.G0", "h1xm.G0", "h1zp.G0",
    "norm1.2", "Ra.0", "Td.1", "mixa.2", "mixb.2", "Rba.3", "h2xp.G0", "Rbb.3",
    "h2zp.G0", "h2zm.G0", "Rx.2", "h3zm.G0", "h3xp.G0", "h3zp.G0", "h3xm.G0", "g1x.G1",
    "fxm.D1", "g3z.G1", "Rbb.0", "Rba.0", "ox.D0", "Ra.2", "g3x.G1", "g1z.G1",
    "norm1.1", "g0z.G1", "g0z.D1", "fzm.D1", "Rc.3", "g0z.D0", "fzp.D0", "Up.3",
    "fzp.D1", "fxp.D1", "g2x.G1", "e.G0", "Rc.0", "g2x.D1", "Up.0", "h1xm.G1",
    "mixa.1", "fxp.D0", "fzm.D0", "g2x.D0", "h0xp.G1", "g3z.D1", "mixb.1", "h0zm.G1",
    "Ufb.3", "g0x.D1", "Ufa.3", "h2xp.G1", "Rx.1", "h3zm.G1", "Rbb.2", "h1xp.G1",
    "fxm.D0", "h3xp.G1", "h2zp.G1", "h1zm.G1", "h1zp.G1", "h3xm.G1", "h2xm.G1", "h0zp.G1",
    "Rba.2", "Ufa.0", "Ufb.0", "h3zp.G1", "h0xm.G1", "g1x.D1", "g1x.D0", "h2zm.G1",
    "g2z.D0", "g2z.D1", "h0zm.D0", "g3x.D1", "g0x.D0", "h2xm.D0", "g3x.D0", "g1z.D0",
    "Ra.1", "h0xm.D1", "g1z.D1", "Ug.3", "g3z.D0", "h2xm.D1", "h0zp.D1", "h0zm.D1",
    "h2xp.D1", "h2xp.D0", "h3zp.D1", "Rc.2", "h3zm.D1", "h0xp.D1", "h0zp.D0", "Up.2",
    "Ud.3", "norm2.3", "Ug.0", "e.G1", "gua.3", "Rba.1", "Rbb.1", "h2zp.D1",
    "h2zm.D1", "h2zp.D0", "h1xp.D0", "h1xm.D1", "h1xm.D0", "Ud.0", "norm2.0", "h1zp.D0",
    "h3xp.D1", "h2zm.D0", "h1zm.D0", "h1xp.D1", "h3xm.D1", "gua.0", "h1zp.D1", "h3xp.D0",
    "h1zm.D1", "h0xp.D0", "h0xm.D0", "h3zp.D0", "h3zm.D0", "h3xm.D0", "Ufa.2", "Ufb.2",
    "gub.3", "Rc.1", "Up.1", "gub.0", "e.D1", "e.D0", "downa.0", "Ug.2",
    "downb.0", "downa.3", "Ud.2", "norm2.2", "Ufa.1", "Ufb.1", "Vx.0", "downb.3",
    "Vx.3", "gua.2", "gub.2", "Va.0", "Va.3", "Ug.1", "downa.2", "downb.2",
    "Ud.1", "norm2.1", "Vx.2", "gua.1", "Vba.0", "Vbb.0", "gub.1", "Va.2",
    "downa.1", "downb.1", "Vx.1", "Vba.3", "Vbb.3", "Vc.0", "Va.1", "Vba.2",
    "Vbb.2", "Vc.3", "Vba.1", "Vbb.1", "Vc.2", "Vc.1",
)


def rope_tables():
    half = DK // 2
    frequency = ROPE_BASE ** (-np.linspace(0.0, 1.0, half))
    angles = np.arange(SEQ)[:, None] * frequency[None, :]
    cosine = np.repeat(np.cos(angles), 2, axis=1)
    sine = np.repeat(np.sin(angles), 2, axis=1) * np.tile([-1.0, 1.0], half)
    scale = DK**-0.5
    return (
        np.concatenate([cosine, cosine * scale], axis=1).astype(np.float32),
        np.concatenate([sine, sine * scale], axis=1).astype(np.float32),
    )


def decay_table():
    rates = np.log1p(-np.exp2(-5.0 - 4.0 * np.arange(HEADS) / (HEADS - 1)))
    return np.broadcast_to(rates[:, None, None], (HEADS, 8, 128)).astype(np.float32)


def silu(values):
    return values / (1.0 + jnp.exp(-values))


def dot(left, right):
    return jnp.dot(left, right, preferred_element_type=F32)


def layer_kernel(
    tok_hbm,
    mix_gain_hbm,
    query_hbm,
    key_hbm,
    value_hbm,
    gate_hbm,
    out_w_hbm,
    head_gain_hbm,
    ffn_gain_hbm,
    ffn_gate_hbm,
    ffn_up_hbm,
    down_hbm,
    cos_hbm,
    sin_hbm,
    rate_hbm,
    out_hbm,
    tok,
    resid,
    normed,
    w_qo,
    w_gu,
    w_d,
    turn_qk,
    turn_gu,
    mix_gain,
    ffn_gain,
    head_gain,
    cos_ref,
    sin_ref,
    rate_ref,
    out_ref,
    mask,
    mixed,
    hidden,
    part1,
    pair1,
    sums1,
    fromp1,
    fromm1,
    relayp1,
    relaym1,
    part2,
    pair2,
    sums2,
    fromp2,
    fromm2,
    relayp2,
    relaym2,
    local_sem,
    send_sem,
    recv_sem,
):
    rep, fs, tp = lax.axis_index("rep"), lax.axis_index("fs"), lax.axis_index("tp")
    y, c = lax.div(tp, 2), lax.rem(tp, 2)
    z, x = lax.div(fs, 4), lax.rem(fs, 4)
    oc = 1 - c

    def step(value, by, size):
        return lax.rem(value + by, size)

    yp, y2, ym = step(y, 1, 4), step(y, 2, 4), step(y, 3, 4)
    xp, x2, xm = step(x, 1, 4), step(x, 2, 4), step(x, 3, 4)
    zp, z2, zm = step(z, 1, 4), step(z, 2, 4), step(z, 3, 4)
    zall = rep * 4 + z

    def z_device(place):
        return (lax.div(place, 4), lax.rem(place, 4) * 4 + x, tp)

    to_yp, to_ym = (rep, fs, yp * 2 + c), (rep, fs, ym * 2 + c)
    to_pt = (rep, fs, y * 2 + oc)
    to_xp, to_xm = (rep, z * 4 + xp, tp), (rep, z * 4 + xm, tp)
    to_zp, to_zm = z_device(step(zall, 1, 8)), z_device(step(zall, 7, 8))

    barrier = pltpu.get_barrier_semaphore()
    peers = (to_yp, to_ym, to_pt, to_xp, to_xm, to_zp, to_zm)
    for peer in peers:
        pl.semaphore_signal(barrier, inc=1, device_id=peer, device_id_type=MESH)

    ids = {}
    sent = []

    def send(key, src, dst, device):
        assert key not in ids
        k = ids[key] = len(ids)
        copy = pltpu.make_async_remote_copy(
            src_ref=src,
            dst_ref=dst,
            send_sem=send_sem.at[k],
            recv_sem=recv_sem.at[k],
            device_id=device,
            device_id_type=MESH,
        )
        copy.start()
        sent.append(copy)

    def recv(key, dst):
        k = ids[key]
        pltpu.make_async_remote_copy(
            src_ref=dst,
            dst_ref=dst,
            send_sem=send_sem.at[k],
            recv_sem=recv_sem.at[k],
            device_id=to_pt,
            device_id_type=MESH,
        ).wait_recv()

    count = [0]

    def local(src, dst):
        copy = pltpu.make_async_copy(src, dst, local_sem.at[count[0]])
        count[0] += 1
        copy.start()
        return copy

    loads = {}
    loads["qk"] = [
        local(query_hbm, turn_qk.at[pl.ds(0, DK)]),
        local(key_hbm, turn_qk.at[pl.ds(DK, DK)]),
    ]
    loads["vgo"] = [
        local(value_hbm, w_qo.at[z, x, :, pl.ds(128, 128)]),
        local(gate_hbm, w_qo.at[z, x, :, pl.ds(256, 128)]),
        local(out_w_hbm, w_qo.at[z, x, :, pl.ds(384, 128)]),
    ]
    loads["tok"] = [local(tok_hbm, tok.at[y, c])]
    loads["gu"] = []
    for j in range(6):
        width = 128 if j < 5 else 64
        for k, source in enumerate((ffn_gate_hbm, ffn_up_hbm)):
            place = pl.ds(256 * j + width * k, width)
            loads["gu"].append(local(source.at[pl.ds(128 * j, width)], turn_gu.at[place]))
    loads["down"] = [local(down_hbm, w_d.at[z, x])]
    loads["rest"] = [
        local(mix_gain_hbm, mix_gain),
        local(ffn_gain_hbm, ffn_gain),
        local(head_gain_hbm, head_gain),
        local(cos_hbm, cos_ref),
        local(sin_hbm, sin_ref),
        local(rate_hbm, rate_ref),
    ]

    def loaded(name):
        for copy in loads[name]:
            copy.wait()

    loaded("qk")
    w_qo[z, x, :, 0:128] = turn_qk[...].T
    loaded("vgo")
    loaded("tok")
    pl.semaphore_wait(barrier, len(peers))

    def stage_gate_up(_):
        loaded("gu")
        for j in range(11):
            lanes = slice(128 * j, 128 * j + 128)
            w_gu[z, x, :, lanes] = turn_gu[lanes, :].T

    def stage_down(_):
        loaded("down")

    def stage_rest(_):
        loaded("rest")
        gap = lax.broadcasted_iota(jnp.int32, (SEQ, 128), 0) - lax.broadcasted_iota(
            jnp.int32, (SEQ, 128), 1
        )
        rate = rate_ref[tp][:1, :]
        for half in range(2):
            distance = (gap - 128 * half).astype(F32)
            mask[:, 128 * half : 128 * half + 128] = jnp.where(
                distance >= 0.0, jnp.exp(jnp.maximum(distance, 0.0) * rate), 0.0
            )

    def rows_of(ch):
        return pl.ds(SEQ * ch, SEQ), pl.ds(SEQ * ch, 128), pl.ds(SEQ * ch + 128, 128)

    def gather_own(buf, tag, ch):
        rows, _, _ = rows_of(ch)
        own = buf.at[y, c, rows]
        send((tag, "yp", ch), own, own, to_yp)
        send((tag, "ym", ch), own, own, to_ym)
        send((tag, "pt0", ch), own, own, to_pt)

    def gather_forward(buf, tag, ch, side):
        rows, low, high = rows_of(ch)
        if side == "a":
            recv((tag, "yp", ch), buf.at[ym, c, rows])
            send((tag, "fp", ch), buf.at[ym, c, low], buf.at[ym, c, low], to_yp)
            send((tag, "pt1", ch), buf.at[ym, c, rows], buf.at[ym, c, rows], to_pt)
        else:
            recv((tag, "ym", ch), buf.at[yp, c, rows])
            send((tag, "fm", ch), buf.at[yp, c, high], buf.at[yp, c, high], to_ym)
            send((tag, "pt2", ch), buf.at[yp, c, rows], buf.at[yp, c, rows], to_pt)

    def gather_far(buf, tag, ch):
        rows, low, high = rows_of(ch)
        recv((tag, "fp", ch), buf.at[y2, c, low])
        recv((tag, "fm", ch), buf.at[y2, c, high])
        send((tag, "pt3", ch), buf.at[y2, c, rows], buf.at[y2, c, rows], to_pt)

    def gather_done(buf, tag, ch):
        rows, _, _ = rows_of(ch)
        recv((tag, "pt0", ch), buf.at[y, oc, rows])
        recv((tag, "pt1", ch), buf.at[ym, oc, rows])
        recv((tag, "pt2", ch), buf.at[yp, oc, rows])
        recv((tag, "pt3", ch), buf.at[y2, oc, rows])

    weight = {"QO": w_qo, "G0": w_gu, "G1": w_gu, "D0": w_d, "D1": w_d}

    def spans(unit):
        first, a, a0, b, b0 = UNITS[unit]
        return (
            pl.ds(first, a),
            pl.ds(first, a0),
            pl.ds(first + a0, a - a0),
            pl.ds(first + a, b),
            pl.ds(first + a, b0),
            pl.ds(first + a + b0, b - b0),
        )

    def near_own(unit, axis):
        w = weight[unit]
        a, _, _, b, _, _ = spans(unit)
        half, plus, minus = (a, to_xp, to_xm) if axis == "x" else (b, to_zp, to_zm)
        send((unit, axis + "p1"), w.at[z, x, half], w.at[z, x, half], plus)
        send((unit, axis + "m1"), w.at[z, x, half], w.at[z, x, half], minus)

    def near_forward(unit, way):
        w = weight[unit]
        a, a0, a1, b, b0, b1 = spans(unit)
        at, half, part, device = {
            "xp": ((z, xm), a, a0, to_xp),
            "xm": ((z, xp), a, a1, to_xm),
            "zp": ((zm, x), b, b0, to_zp),
            "zm": ((zp, x), b, b1, to_zm),
        }[way]
        recv((unit, way + "1"), w.at[(*at, half)])
        send((unit, way + "f1"), w.at[(*at, part)], w.at[(*at, part)], device)

    places = {"z": (x, xm, xp, x2), "x": (z, zm, zp, z2)}

    def far_at(axis, row, i):
        return (row, places["z"][i]) if axis == "z" else (places["x"][i], row)

    def far_own(unit, axis, i):
        w = weight[unit]
        a, a0, a1, b, b0, b1 = spans(unit)
        if axis == "z":
            at, half, plus, minus = far_at("z", z, i), a, to_zp, to_zm
        else:
            at, half, plus, minus = far_at("x", x, i), b, to_xp, to_xm
        if i == 3:
            first, low, high = ("x", a0, a1) if axis == "z" else ("z", b0, b1)
            recv((unit, first + "pf1"), w.at[(*at, low)])
            recv((unit, first + "mf1"), w.at[(*at, high)])
        send((unit, axis + "p2", i), w.at[(*at, half)], w.at[(*at, half)], plus)
        send((unit, axis + "m2", i), w.at[(*at, half)], w.at[(*at, half)], minus)

    def far_forward(unit, way, i):
        w = weight[unit]
        a, a0, a1, b, b0, b1 = spans(unit)
        row, half, part, device = {
            "zp": (zm, a, a0, to_zp),
            "zm": (zp, a, a1, to_zm),
            "xp": (xm, b, b0, to_xp),
            "xm": (xp, b, b1, to_xm),
        }[way]
        at = far_at(way[0], row, i)
        recv((unit, way + "2", i), w.at[(*at, half)])
        send((unit, way + "f2", i), w.at[(*at, part)], w.at[(*at, part)], device)

    def weight_done(unit):
        w = weight[unit]
        a, a0, a1, b, b0, b1 = spans(unit)
        for i in range(4):
            recv((unit, "zpf2", i), w.at[(*far_at("z", z2, i), a0)])
            recv((unit, "zmf2", i), w.at[(*far_at("z", z2, i), a1)])
            recv((unit, "xpf2", i), w.at[(*far_at("x", x2, i), b0)])
            recv((unit, "xmf2", i), w.at[(*far_at("x", x2, i), b1)])

    mixer_bufs = (part1, pair1, sums1, fromp1, fromm1, relayp1, relaym1)
    ffn_bufs = (part2, pair2, sums2, fromp2, fromm2, relayp2, relaym2)

    def sum_pair(bufs, tag, ch):
        part, pair = bufs[:2]
        rows, _, _ = rows_of(ch)
        send((tag, "pair", ch), part.at[oc, :, rows], pair.at[:, rows], to_pt)

    def sum_start(bufs, tag, ch):
        part, pair, sums, fromp, fromm, relayp, relaym = bufs
        rows, low, high = rows_of(ch)
        half = pl.ds(128 * ch, 128)
        recv((tag, "pair", ch), pair.at[:, rows])
        for place in (y2, yp, ym):
            sums[place, rows] = (
                part[c, place, rows].astype(F32) + pair[place, rows].astype(F32)
            ).astype(BF16)
        send((tag, "rp", ch), sums.at[y2, low], relayp.at[half], to_yp)
        send((tag, "rm", ch), sums.at[y2, high], relaym.at[half], to_ym)
        send((tag, "op", ch), sums.at[yp, high], fromm.at[high], to_yp)
        send((tag, "om", ch), sums.at[ym, low], fromp.at[low], to_ym)

    def sum_relay(bufs, tag, ch, side):
        part, pair, sums, fromp, fromm, relayp, relaym = bufs
        rows, low, high = rows_of(ch)
        half = pl.ds(128 * ch, 128)
        if side == "a":
            recv((tag, "rp", ch), relayp.at[half])
            sums[yp, low] = (sums[yp, low].astype(F32) + relayp[half].astype(F32)).astype(BF16)
            send((tag, "sp", ch), sums.at[yp, low], fromm.at[low], to_yp)
        else:
            recv((tag, "rm", ch), relaym.at[half])
            sums[ym, high] = (sums[ym, high].astype(F32) + relaym[half].astype(F32)).astype(BF16)
            send((tag, "sm", ch), sums.at[ym, high], fromp.at[high], to_ym)

    def sum_end(bufs, tag, ch):
        part, pair, sums, fromp, fromm, relayp, relaym = bufs
        rows, low, high = rows_of(ch)
        recv((tag, "op", ch), fromm.at[high])
        recv((tag, "om", ch), fromp.at[low])
        recv((tag, "sp", ch), fromm.at[low])
        recv((tag, "sm", ch), fromp.at[high])
        return (part[c, y, rows].astype(F32) + pair[y, rows].astype(F32)) + (
            fromp[rows].astype(F32) + fromm[rows].astype(F32)
        )

    stores = []

    def mixer_end(ch):
        rows, _, _ = rows_of(ch)
        total = sum_end(mixer_bufs, "R", ch)
        resid[y, c, rows] = (tok[y, c, rows].astype(F32) + total).astype(BF16)

    def ffn_end(ch):
        rows, _, _ = rows_of(ch)
        total = sum_end(ffn_bufs, "V", ch)
        out_ref[rows, :] = (resid[y, c, rows].astype(F32) + total).astype(BF16)
        stores.append(local(out_ref.at[rows], out_hbm.at[rows]))

    def norm_rows(buf, gain, ch):
        def body(i, carry):
            rows = pl.ds(pl.multiple_of(SEQ * ch + 32 * i, 32), 32)
            blocks = [buf[p // 2, p % 2, rows].astype(F32) for p in range(8)]
            squares = blocks[0] * blocks[0]
            for block in blocks[1:]:
                squares = squares + block * block
            mean = jnp.sum(squares, axis=-1, keepdims=True) * (1.0 / 2048.0)
            factor = lax.rsqrt(mean + EPS)
            for p in range(8):
                lanes = slice(256 * p, 256 * p + 256)
                normed[rows, lanes] = (blocks[p] * factor * gain[:, lanes]).astype(BF16)
            return carry

        lax.fori_loop(0, 8, body, 0)

    def mixer(ch):
        rows, _, _ = rows_of(ch)
        qkv = dot(normed[rows, :], w_qo[:, :, :, 0:256].reshape(2048, 256))
        gate = dot(normed[rows, :], w_qo[:, :, :, 256:384].reshape(2048, 128))
        gate = gate.astype(BF16).astype(F32)
        qk = qkv[:, :128].astype(BF16).astype(F32)
        value = qkv[:, 128:].astype(BF16)
        lane = lax.broadcasted_iota(jnp.int32, (SEQ, 128), 1)
        turned = jnp.where(
            lax.rem(lane, 2) == 0, pltpu.roll(qk, 127, axis=1), pltpu.roll(qk, 1, axis=1)
        )
        rotated = qk * cos_ref[...] + turned * sin_ref[...]
        queries = jnp.where(lane < DK, rotated, 0.0).astype(BF16)
        keys = pltpu.roll(rotated, DK, axis=1).astype(BF16)
        scores = lax.dot_general(
            queries, keys, (((1,), (1,)), ((), ())), preferred_element_type=F32
        )
        retained = dot((scores * mask[...]).astype(BF16), value)
        center = jnp.mean(retained, axis=-1, keepdims=True)
        moved = retained - center
        spread = jnp.mean(moved * moved, axis=-1, keepdims=True)
        grouped = moved * lax.rsqrt(spread + EPS) * head_gain[...]
        mixed[rows] = (grouped * silu(gate)).astype(BF16)

    def mixer_out(ch):
        rows, _, _ = rows_of(ch)

        def body(p, carry):
            py, pc = lax.div(p, 2), lax.rem(p, 2)
            block = jnp.concatenate(
                [w_qo[py, 2 * pc, :, 384:512], w_qo[py, 2 * pc + 1, :, 384:512]], axis=1
            )
            part1[pc, py, rows] = dot(mixed[rows], block).astype(BF16)
            return carry

        lax.fori_loop(0, 8, body, 0)

    def gate_up(ch, first):
        rows, _, _ = rows_of(ch)

        def body(j, carry):
            columns = pl.ds(pl.multiple_of(256 * j, 256), 256)
            both = dot(normed[rows, :], w_gu[:, :, :, columns].reshape(2048, 256))
            hidden[rows, pl.ds(pl.multiple_of(128 * j, 128), 128)] = (
                silu(both[:, :128]) * both[:, 128:]
            ).astype(BF16)
            return carry

        if first:
            lax.fori_loop(0, 3, body, 0)
            return
        lax.fori_loop(3, 5, body, 0)
        both = dot(normed[rows, :], w_gu[:, :, :, 1280:1408].reshape(2048, 128))
        hidden[rows, 640:768] = (silu(both) * pltpu.roll(both, 64, axis=1)).astype(BF16)

    def down(ch, first):
        rows, _, _ = rows_of(ch)

        def body(p, carry):
            py, pc = lax.div(p, 2), lax.rem(p, 2)
            block = jnp.concatenate([w_d[py, 2 * pc], w_d[py, 2 * pc + 1]], axis=1)
            part2[pc, py, rows] = dot(hidden[rows, :704], block).astype(BF16)
            return carry

        lax.fori_loop(*((0, 4) if first else (4, 8)), body, 0)

    actions = {
        "ox": lambda u: near_own(u, "x"),
        "oz": lambda u: near_own(u, "z"),
        "e": weight_done,
        "stage_gu": stage_gate_up,
        "stage_d": stage_down,
        "stage_c": stage_rest,
        "Rc": mixer_end,
        "Vc": ffn_end,
        "norm1": lambda ch: norm_rows(tok, mix_gain, ch),
        "norm2": lambda ch: norm_rows(resid, ffn_gain, ch),
        "mixa": mixer,
        "mixb": mixer_out,
        "gua": functools.partial(gate_up, first=True),
        "gub": functools.partial(gate_up, first=False),
        "downa": functools.partial(down, first=True),
        "downb": functools.partial(down, first=False),
    }
    for way in ("xp", "xm", "zp", "zm"):
        actions["f" + way] = functools.partial(near_forward, way=way)
        for i in range(4):
            actions[f"h{i}" + way] = functools.partial(far_forward, way=way, i=i)
    for i in range(4):
        actions[f"g{i}z"] = functools.partial(far_own, axis="z", i=i)
        actions[f"g{i}x"] = functools.partial(far_own, axis="x", i=i)
    for tag, buf in (("T", tok), ("U", resid)):
        actions[tag + "p"] = functools.partial(gather_own, buf, tag)
        actions[tag + "fa"] = functools.partial(gather_forward, buf, tag, side="a")
        actions[tag + "fb"] = functools.partial(gather_forward, buf, tag, side="b")
        actions[tag + "g"] = functools.partial(gather_far, buf, tag)
        actions[tag + "d"] = functools.partial(gather_done, buf, tag)
    for tag, bufs in (("R", mixer_bufs), ("V", ffn_bufs)):
        actions[tag + "x"] = functools.partial(sum_pair, bufs, tag)
        actions[tag + "a"] = functools.partial(sum_start, bufs, tag)
        actions[tag + "ba"] = functools.partial(sum_relay, bufs, tag, side="a")
        actions[tag + "bb"] = functools.partial(sum_relay, bufs, tag, side="b")
    for entry in SCHEDULE:
        name, what = entry.split(".")
        actions[name](int(what) if what.isdigit() else what)

    for copy in sent:
        copy.wait_send()
    for copy in stores:
        copy.wait()
    assert len(ids) <= MAX_COPIES


def per_device(*args):
    (tokens, mix_gain, query_w, key_w, value_w, gate_w, out_w, head_gain, ffn_gain) = args[:9]
    ffn_gate, ffn_up, ffn_down = args[9:]
    cosine, sine = rope_tables()
    hbm = pl.BlockSpec(memory_space=pltpu.HBM)
    rows = tokens.shape[0]

    def sum_buffers():
        return [
            pltpu.VMEM((2, 4, rows, 256), BF16),
            pltpu.VMEM((4, rows, 256), BF16),
            pltpu.VMEM((4, rows, 256), BF16),
            pltpu.VMEM((rows, 256), BF16),
            pltpu.VMEM((rows, 256), BF16),
            pltpu.VMEM((rows // 2, 256), BF16),
            pltpu.VMEM((rows // 2, 256), BF16),
        ]

    call = pl.pallas_call(
        layer_kernel,
        out_shape=jax.ShapeDtypeStruct((rows, 256), BF16),
        in_specs=[hbm] * 15,
        out_specs=hbm,
        scratch_shapes=[
            pltpu.VMEM((4, 2, rows, 256), BF16),
            pltpu.VMEM((4, 2, rows, 256), BF16),
            pltpu.VMEM((rows, 2048), BF16),
            pltpu.VMEM((4, 4, 128, 512), BF16),
            pltpu.VMEM((4, 4, 128, 1408), BF16),
            pltpu.VMEM((4, 4, 704, 128), BF16),
            pltpu.VMEM((2 * DK, 128), BF16),
            pltpu.VMEM((1408, 128), BF16),
            pltpu.VMEM((1, 2048), F32),
            pltpu.VMEM((1, 2048), F32),
            pltpu.VMEM((1, DV), F32),
            pltpu.VMEM((SEQ, 128), F32),
            pltpu.VMEM((SEQ, 128), F32),
            pltpu.VMEM((HEADS, 8, 128), F32),
            pltpu.VMEM((rows, 256), BF16),
            pltpu.VMEM((SEQ, SEQ), F32),
            pltpu.VMEM((rows, DV), BF16),
            pltpu.VMEM((rows, 768), BF16),
            *sum_buffers(),
            *sum_buffers(),
            pltpu.SemaphoreType.DMA((32,)),
            pltpu.SemaphoreType.DMA((MAX_COPIES,)),
            pltpu.SemaphoreType.DMA((MAX_COPIES,)),
        ],
        compiler_params=pltpu.CompilerParams(
            collective_id=0, has_side_effects=True, vmem_limit_bytes=54 * 2**20
        ),
        cost_estimate=pl.CostEstimate(
            flops=11_000_000_000, bytes_accessed=4_000_000, transcendentals=1_000_000
        ),
        name="layer",
    )
    return call(
        tokens,
        mix_gain.reshape(1, -1),
        query_w.T,
        key_w.T,
        value_w,
        gate_w,
        out_w,
        head_gain,
        ffn_gain.reshape(1, -1),
        ffn_gate.T,
        ffn_up.T,
        ffn_down,
        jnp.asarray(cosine),
        jnp.asarray(sine),
        jnp.asarray(decay_table()),
    )


def solution(mesh):
    placed = (
        P(("rep", "fs"), "tp"),
        P(),
        P("fs", "tp"),
        P("fs", "tp"),
        P("fs", "tp"),
        P("fs", "tp"),
        P("tp", "fs"),
        P("tp", None),
        P(),
        P("fs", "tp"),
        P("fs", "tp"),
        P("tp", "fs"),
    )
    return jax.shard_map(
        per_device, mesh=mesh, in_specs=placed, out_specs=P(("rep", "fs"), "tp"), check_vma=False
    )
```

time: 385 us -> 102 us (0.26)
  blocking collectives: 174 us -> 0 us
  waiting for transfers between devices: 106 us -> 0 us
  Pallas kernels: 0 us -> 100 us
  matrix products: 37.9 us -> 0 us
  local copies, waits for them, and re-layouts: 31.7 us -> 1.87 us
  other arithmetic: 15.5 us -> 0 us
  between operations: 13.9 us -> 0.01 us
  starting transfers between devices: 4.38 us -> 0 us
    all_to_all x2 -> x0, blocking collectives: 116 us -> none  [sent_and_summed(): pieces = lax.all_to_all(cut_along(array, dim, size), axis, 0, 0, tiled=True)]
    all_gather x6 -> x0, waiting for transfers between devices: 105 us -> none  [the longest x1 43.1 us: in_one_piece(): out = lax.all_gather(both, axis, axis=dim, tiled=True)]
    pallas_call x0 -> x1, Pallas kernels: none -> 100 us  [per_device(): call(tokens, mix_gain.reshape(1, -1), query_w.T, key_w.T, value_w, gate_w...]
    all_gather x3 -> x0, blocking collectives: 58.3 us -> none  [gather_in_order(): pieces = lax.all_gather(pieces, axes[k], axis=0, tiled=True)]
    dot_general x23 -> x0, matrix products: 37.9 us -> none  [the longest x4 13.8 us: per_device(): jnp.dot(normed, weight_piece, preferred_element_type=jnp.float32)]
    transpose x4 -> x0, local copies, waits for them, and re-layouts: 12 us -> none  [the longest x3 11.9 us: gather_in_order(): pieces.transpose(*turned, *range(len(order), pieces.ndim))]
    reduce_sum x6 -> x0, other arithmetic: 8.22 us -> none  [the longest x2 6.45 us: norm_rows(): jnp.mean(floats * floats, axis=-1, keepdims=True) + epsilon]
    another operation x6 -> x0, local copies, waits for them, and re-layouts: 7.77 us -> none  [the longest x2 6.83 us: joined_along(): return jnp.moveaxis(pieces, 0, dim).reshape(shape)]
  transfers between devices with their start and end apart: 7 -> 0, of which waited for: 3 -> 0; matrix products, arithmetic and copies ran while one was open for 15% -> 0% of each run, Pallas kernels for 0% -> 0%
where the time goes in v1:
time: 102 us
  Pallas kernels  100 us (98%)
  local copies, waits for them, and re-layouts  1.87 us (2%)
    pallas_call x1, Pallas kernels, per_device(): call(tokens, mix_gain.reshape(1, -1), query_w.T, key_w.T, value_w, gate_w...  100 us

profile of v1, /device:TPU:1, one launch (start us, length us, event | category | flops | bytes accessed | tf_op | source)
XLA Modules:
  0.0 102.2 jit_solution(3633924412867589541)
XLA Ops:
  0.0 100.3 %layer.1 = bf16[1024,256]{1,0:T(8,128)(2,1)} custom-call(bf16[1024,256]{1,0:T(8,128)(2,1)} %tok_hbm.1, f32[1,2048]{1,0:T(1,128)} %bitcast.10, bf16[64,128]{1,0:T(8,128)(2,1)} %bitcast.8, bf16[64,128]{1,0:T(8,128)(2,1)} %bitcast.9, bf16[128,128]{1,0:T(8,128)(2,1)} %value_hbm.1, bf16[128,128]{1,0:T(8,128)(2,1)} %gate_hbm.1, bf16[128,128]{1,0:T(8,128)(2,1)} %out_w_hbm.1, ...), custom_call_target="tpu_custom_call" | custom-call | flops 11000000512 | bytes 4000000 | tf_op jit(solution)/shard_map/layer/pallas_call | solution.py:618
  100.3 1.9 %copy.17 = bf16[1024,256]{1,0:T(8,128)(2,1)} copy(bf16[1024,256]{1,0:T(8,128)(2,1)} %layer.1) | data formatting | bytes 1048576

commit v2 on v1

v2 whole, which is shorter than its diff:
```python
import functools

import jax
import jax.numpy as jnp
import numpy as np
from jax import lax
from jax.experimental import pallas as pl
from jax.experimental.pallas import tpu as pltpu
from jax.sharding import PartitionSpec as P

HEADS = 8
DK = 64
DV = 128
SEQ = 256
EPS = 1e-06
ROPE_BASE = 10000.0
F32 = jnp.float32
BF16 = jnp.bfloat16
MESH = pl.DeviceIdType.MESH
RECEIVES = 179
SENDS = 14

UNITS = (
    (0, 64, 32, 64, 32),
    (0, 32, 16, 32, 16),
    (64, 32, 16, 32, 16),
    (0, 176, 96, 176, 96),
    (352, 176, 96, 176, 96),
)
WEIGHT_OF = (0, 1, 1, 2, 2)

SCHEDULE = (
    8, 0, 274, 48, 248, 275, 80, 10, 2, 272, 40, 32, 24, 16, 64, 96,
    282, 290, 144, 112, 176, 56, 208, 256, 88, 104, 72, 291, 9, 1, 283, 280,
    288, 273, 264, 192, 216, 120, 128, 184, 160, 224, 152, 298, 200, 232, 168, 136,
    82, 299, 4, 50, 26, 42, 34, 66, 306, 434, 18, 12, 33, 90, 307, 11,
    296, 435, 25, 41, 98, 58, 240, 443, 451, 355, 281, 304, 17, 289, 442, 106,
    450, 354, 363, 81, 74, 432, 210, 440, 297, 44, 362, 36, 448, 194, 130, 146,
    52, 352, 162, 305, 154, 114, 122, 3, 178, 35, 371, 379, 226, 218, 360, 43,
    202, 186, 433, 170, 138, 234, 378, 370, 20, 97, 57, 51, 441, 387, 65, 105,
    315, 449, 376, 19, 27, 353, 49, 28, 83, 242, 368, 89, 59, 386, 99, 68,
    314, 361, 108, 67, 323, 73, 107, 91, 75, 100, 384, 115, 153, 92, 217, 331,
    193, 76, 113, 60, 201, 233, 121, 225, 148, 322, 330, 377, 369, 84, 137, 161,
    169, 185, 312, 145, 177, 339, 236, 209, 228, 211, 171, 147, 187, 204, 129, 163,
    123, 227, 139, 219, 131, 155, 338, 195, 347, 179, 235, 220, 203, 164, 116, 132,
    385, 313, 346, 196, 124, 156, 172, 188, 180, 140, 459, 212, 458, 241, 320, 328,
    467, 466, 243, 475, 244, 483, 329, 321, 491, 395, 474, 336, 482, 490, 394, 403,
    344, 456, 464, 337, 402, 472, 480, 488, 392, 345, 457, 419, 411, 465, 400, 473,
    481, 489, 393, 418, 410, 427, 401, 408, 416, 426, 417, 409, 424, 425,
)


def rope_tables():
    half = DK // 2
    frequency = ROPE_BASE ** (-np.linspace(0.0, 1.0, half))
    angles = np.arange(SEQ)[:, None] * frequency[None, :]
    cosine = np.repeat(np.cos(angles), 2, axis=1)
    sine = np.repeat(np.sin(angles), 2, axis=1) * np.tile([-1.0, 1.0], half)
    scale = DK**-0.5
    return (
        np.concatenate([cosine, cosine * scale], axis=1).astype(np.float32),
        np.concatenate([sine, sine * scale], axis=1).astype(np.float32),
    )


def decay_table():
    rates = np.log1p(-np.exp2(-5.0 - 4.0 * np.arange(HEADS) / (HEADS - 1)))
    return np.broadcast_to(rates[:, None, None], (HEADS, 8, 128)).astype(np.float32)


def silu(values):
    return values / (1.0 + jnp.exp(-values))


def dot(left, right):
    return jnp.dot(left, right, preferred_element_type=F32)


def layer_kernel(
    tok_hbm,
    mix_gain_hbm,
    query_hbm,
    key_hbm,
    value_hbm,
    gate_hbm,
    out_w_hbm,
    head_gain_hbm,
    ffn_gain_hbm,
    ffn_gate_hbm,
    ffn_up_hbm,
    down_hbm,
    cos_hbm,
    sin_hbm,
    rate_hbm,
    out_hbm,
    tok,
    resid,
    normed,
    w_qo,
    w_gu,
    w_d,
    turn_qk,
    turn_gu,
    mix_gain,
    ffn_gain,
    head_gain,
    cos_ref,
    sin_ref,
    rate_ref,
    out_ref,
    mask,
    mixed,
    hidden,
    part1,
    pair1,
    sums1,
    ends1,
    relay1,
    part2,
    pair2,
    sums2,
    ends2,
    relay2,
    local_sem,
    send_sem,
    recv_sem,
):
    rep, fs, tp = lax.axis_index("rep"), lax.axis_index("fs"), lax.axis_index("tp")
    y, c = lax.div(tp, 2), lax.rem(tp, 2)
    z, x = lax.div(fs, 4), lax.rem(fs, 4)
    oc = 1 - c

    def step(value, by, size):
        return lax.rem(value + by, size)

    yp, y2, ym = step(y, 1, 4), step(y, 2, 4), step(y, 3, 4)
    xp, x2, xm = step(x, 1, 4), step(x, 2, 4), step(x, 3, 4)
    zp, z2, zm = step(z, 1, 4), step(z, 2, 4), step(z, 3, 4)
    zall = rep * 4 + z

    def z_device(place):
        return (lax.div(place, 4), lax.rem(place, 4) * 4 + x, tp)

    to_yp, to_ym = (rep, fs, yp * 2 + c), (rep, fs, ym * 2 + c)
    to_pt = (rep, fs, y * 2 + oc)
    to_xp, to_xm = (rep, z * 4 + xp, tp), (rep, z * 4 + xm, tp)
    to_zp, to_zm = z_device(step(zall, 1, 8)), z_device(step(zall, 7, 8))

    barrier = pltpu.get_barrier_semaphore()
    peers = (to_yp, to_ym, to_pt, to_xp, to_xm, to_zp, to_zm)
    for peer in peers:
        pl.semaphore_signal(barrier, inc=1, device_id=peer, device_id_type=MESH)

    ids = {}
    groups = {}

    def send(group, key, src, dst, device):
        k = ids.setdefault(key, len(ids))
        g = groups.setdefault(group, len(groups))
        pltpu.make_async_remote_copy(
            src_ref=src,
            dst_ref=dst,
            send_sem=send_sem.at[g],
            recv_sem=recv_sem.at[k],
            device_id=device,
            device_id_type=MESH,
        ).start()

    def recv(key, dst):
        pltpu.make_async_remote_copy(
            src_ref=dst,
            dst_ref=dst,
            send_sem=send_sem.at[0],
            recv_sem=recv_sem.at[ids[key]],
            device_id=to_pt,
            device_id_type=MESH,
        ).wait_recv()

    def all_sent(group, src):
        pltpu.make_async_remote_copy(
            src_ref=src,
            dst_ref=src,
            send_sem=send_sem.at[groups[group]],
            recv_sem=recv_sem.at[0],
            device_id=to_pt,
            device_id_type=MESH,
        ).wait_send()

    count = [0]

    def local(src, dst):
        copy = pltpu.make_async_copy(src, dst, local_sem.at[count[0]])
        count[0] += 1
        copy.start()
        return copy

    load_qk = [
        local(query_hbm, turn_qk.at[pl.ds(0, DK)]),
        local(key_hbm, turn_qk.at[pl.ds(DK, DK)]),
    ]
    load_vgo = [
        local(value_hbm, w_qo.at[z, x, :, pl.ds(128, 128)]),
        local(gate_hbm, w_qo.at[z, x, :, pl.ds(256, 128)]),
        local(out_w_hbm, w_qo.at[z, x, :, pl.ds(384, 128)]),
    ]
    load_tok = [local(tok_hbm, tok.at[y, c])]
    load_gu = []
    for j in range(6):
        width = 128 if j < 5 else 64
        for k, source in enumerate((ffn_gate_hbm, ffn_up_hbm)):
            place = pl.ds(256 * j + width * k, width)
            load_gu.append(local(source.at[pl.ds(128 * j, width)], turn_gu.at[place]))
    load_down = [local(down_hbm, w_d.at[z, x])]
    load_rest = [
        local(mix_gain_hbm, mix_gain),
        local(ffn_gain_hbm, ffn_gain),
        local(head_gain_hbm, head_gain),
        local(cos_hbm, cos_ref),
        local(sin_hbm, sin_ref),
        local(rate_hbm, rate_ref),
    ]

    def loaded(copies):
        for copy in copies:
            copy.wait()

    loaded(load_qk)
    w_qo[z, x, :, 0:128] = turn_qk[...].T
    loaded(load_vgo)
    loaded(load_tok)
    pl.semaphore_wait(barrier, len(peers))

    def stage_gate_up(_):
        loaded(load_gu)
        for j in range(11):
            lanes = slice(128 * j, 128 * j + 128)
            w_gu[z, x, :, lanes] = turn_gu[lanes, :].T

    def stage_down(_):
        loaded(load_down)

    def stage_rest(_):
        loaded(load_rest)
        gap = lax.broadcasted_iota(jnp.int32, (SEQ, 128), 0) - lax.broadcasted_iota(
            jnp.int32, (SEQ, 128), 1
        )
        rate = rate_ref[tp][:1, :]
        for half in range(2):
            distance = (gap - 128 * half).astype(F32)
            mask[:, 128 * half : 128 * half + 128] = jnp.where(
                distance >= 0.0, jnp.exp(jnp.maximum(distance, 0.0) * rate), 0.0
            )

    def rows_of(ch):
        return pl.ds(SEQ * ch, SEQ), pl.ds(SEQ * ch, 128), pl.ds(SEQ * ch + 128, 128)

    def gather_own(buf, tag, ch):
        rows, _, _ = rows_of(ch)
        own = buf.at[y, c, rows]
        send((tag, 0), (tag, 0, ch), own, own, to_yp)
        send((tag, 0), (tag, 1, ch), own, own, to_ym)
        send((tag, 1), (tag, 3, ch), own, own, to_pt)

    def gather_forward(buf, tag, ch, side):
        rows, low, high = rows_of(ch)
        row, part, device = ((ym, low, to_yp), (yp, high, to_ym))[side]
        recv((tag, side, ch), buf.at[row, c, rows])
        send((tag, 0), (tag, 2, ch), buf.at[row, c, part], buf.at[row, c, part], device)
        send((tag, 1), (tag, 3, ch), buf.at[row, c, rows], buf.at[row, c, rows], to_pt)

    def gather_far(buf, tag, ch):
        rows, _, _ = rows_of(ch)
        recv((tag, 2, ch), buf.at[y2, c, rows])
        send((tag, 1), (tag, 3, ch), buf.at[y2, c, rows], buf.at[y2, c, rows], to_pt)

    def gather_done(buf, tag, ch):
        rows, _, _ = rows_of(ch)
        recv((tag, 3, ch), buf.at[:, oc, rows])

    buffers = (w_qo, w_gu, w_gu, w_d, w_d)

    def spans(unit):
        first, a, a0, b, b0 = UNITS[unit]
        half_a = (pl.ds(first, a), pl.ds(first, a0), pl.ds(first + a0, a - a0))
        first = first + a
        return half_a, (pl.ds(first, b), pl.ds(first, b0), pl.ds(first + b0, b - b0))

    near = ((xm, xp), (zm, zp))
    far = (x2, z2)
    devices = ((to_xp, to_xm), (to_zp, to_zm))

    def near_at(axis, place):
        return (z, place) if axis == 0 else (place, x)

    def near_own(unit, axis):
        w, name = buffers[unit], WEIGHT_OF[unit]
        half = spans(unit)[axis][0]
        own = w.at[z, x, half]
        for way in range(2):
            send((name, 0), (unit, 0, axis, way), own, own, devices[axis][way])

    def near_forward(unit, axis, way):
        w, name = buffers[unit], WEIGHT_OF[unit]
        at = near_at(axis, near[axis][way])
        half = spans(unit)[axis]
        recv((unit, 0, axis, way), w.at[(*at, half[0])])
        part = w.at[(*at, half[1 + way])]
        send((name, 0), (unit, 1, axis), part, part, devices[axis][way])

    crossed = ((x, xm, xp, x2), (z, zm, zp, z2))

    def far_at(axis, place, i):
        return (place, crossed[0][i]) if axis == 0 else (crossed[1][i], place)

    def far_own(unit, axis, i):
        w, name = buffers[unit], WEIGHT_OF[unit]
        half = spans(unit)[axis][0]
        block = w.at[(*far_at(axis, (z, x)[axis], i), half)]
        if i == 3:
            recv((unit, 1, axis), block)
        for way in range(2):
            send((name, 1), (unit, 2, axis, way, i), block, block, devices[1 - axis][way])

    def far_forward(unit, axis, way, i):
        w, name = buffers[unit], WEIGHT_OF[unit]
        at = far_at(axis, near[1 - axis][way], i)
        half = spans(unit)[axis]
        recv((unit, 2, axis, way, i), w.at[(*at, half[0])])
        part = w.at[(*at, half[1 + way])]
        send((name, 1), (unit, 3), part, part, devices[1 - axis][way])

    def weight_done(unit):
        first, a, _, b, _ = UNITS[unit]
        recv((unit, 3), buffers[unit].at[0, :, pl.ds(first, a + b)])

    mixer_bufs = (part1, pair1, sums1, ends1, relay1)
    ffn_bufs = (part2, pair2, sums2, ends2, relay2)

    def sum_pair(bufs, tag, ch):
        part, pair = bufs[:2]
        rows, _, _ = rows_of(ch)
        send((tag, 1), (tag, 0, ch), part.at[oc, :, rows], pair.at[:, rows], to_pt)

    def sum_start(bufs, tag, ch):
        part, pair, sums, ends, relay = bufs
        rows, low, high = rows_of(ch)
        half = pl.ds(128 * ch, 128)
        recv((tag, 0, ch), pair.at[:, rows])
        for place in (y2, yp, ym):
            sums[place, rows] = (
                part[c, place, rows].astype(F32) + pair[place, rows].astype(F32)
            ).astype(BF16)
        send((tag, 0), (tag, 1, ch), sums.at[y2, low], relay.at[0, half], to_yp)
        send((tag, 0), (tag, 2, ch), sums.at[y2, high], relay.at[1, half], to_ym)
        send((tag, 0), (tag, 3, ch), sums.at[yp, high], ends.at[1, high], to_yp)
        send((tag, 0), (tag, 3, ch), sums.at[ym, low], ends.at[0, low], to_ym)

    def sum_relay(bufs, tag, ch, side):
        _, _, sums, ends, relay = bufs
        _, low, high = rows_of(ch)
        half = pl.ds(128 * ch, 128)
        place, part, device = ((yp, low, to_yp), (ym, high, to_ym))[side]
        recv((tag, 1 + side, ch), relay.at[side, half])
        sums[place, part] = (
            sums[place, part].astype(F32) + relay[side, half].astype(F32)
        ).astype(BF16)
        send((tag, 0), (tag, 3, ch), sums.at[place, part], ends.at[1 - side, part], device)

    def sum_end(bufs, tag, ch):
        part, pair, _, ends, _ = bufs
        rows, _, _ = rows_of(ch)
        recv((tag, 3, ch), ends.at[:, rows])
        return (part[c, y, rows].astype(F32) + pair[y, rows].astype(F32)) + (
            ends[0, rows].astype(F32) + ends[1, rows].astype(F32)
        )

    stores = []

    def mixer_end(ch):
        rows, _, _ = rows_of(ch)
        total = sum_end(mixer_bufs, 12, ch)
        resid[y, c, rows] = (tok[y, c, rows].astype(F32) + total).astype(BF16)

    def ffn_end(ch):
        rows, _, _ = rows_of(ch)
        total = sum_end(ffn_bufs, 13, ch)
        out_ref[rows, :] = (resid[y, c, rows].astype(F32) + total).astype(BF16)
        stores.append(local(out_ref.at[rows], out_hbm.at[rows]))

    def norm_rows(buf, gain, ch):
        def body(i, carry):
            rows = pl.ds(pl.multiple_of(SEQ * ch + 32 * i, 32), 32)
            blocks = [buf[p // 2, p % 2, rows].astype(F32) for p in range(8)]
            squares = blocks[0] * blocks[0]
            for block in blocks[1:]:
                squares = squares + block * block
            mean = jnp.sum(squares, axis=-1, keepdims=True) * (1.0 / 2048.0)
            factor = lax.rsqrt(mean + EPS)
            for p in range(8):
                lanes = slice(256 * p, 256 * p + 256)
                normed[rows, lanes] = (blocks[p] * factor * gain[:, lanes]).astype(BF16)
            return carry

        lax.fori_loop(0, 8, body, 0)

    def mixer(ch):
        rows, _, _ = rows_of(ch)
        qkv = dot(normed[rows, :], w_qo[:, :, :, 0:256].reshape(2048, 256))
        gate = dot(normed[rows, :], w_qo[:, :, :, 256:384].reshape(2048, 128))
        gate = gate.astype(BF16).astype(F32)
        qk = qkv[:, :128].astype(BF16).astype(F32)
        value = qkv[:, 128:].astype(BF16)
        lane = lax.broadcasted_iota(jnp.int32, (SEQ, 128), 1)
        turned = jnp.where(
            lax.rem(lane, 2) == 0, pltpu.roll(qk, 127, axis=1), pltpu.roll(qk, 1, axis=1)
        )
        rotated = qk * cos_ref[...] + turned * sin_ref[...]
        queries = jnp.where(lane < DK, rotated, 0.0).astype(BF16)
        keys = pltpu.roll(rotated, DK, axis=1).astype(BF16)
        scores = lax.dot_general(
            queries, keys, (((1,), (1,)), ((), ())), preferred_element_type=F32
        )
        retained = dot((scores * mask[...]).astype(BF16), value)
        center = jnp.mean(retained, axis=-1, keepdims=True)
        moved = retained - center
        spread = jnp.mean(moved * moved, axis=-1, keepdims=True)
        grouped = moved * lax.rsqrt(spread + EPS) * head_gain[...]
        mixed[rows] = (grouped * silu(gate)).astype(BF16)

    def mixer_out(ch):
        rows, _, _ = rows_of(ch)

        def body(p, carry):
            py, pc = lax.div(p, 2), lax.rem(p, 2)
            block = jnp.concatenate(
                [w_qo[py, 2 * pc, :, 384:512], w_qo[py, 2 * pc + 1, :, 384:512]], axis=1
            )
            part1[pc, py, rows] = dot(mixed[rows], block).astype(BF16)
            return carry

        lax.fori_loop(0, 8, body, 0, unroll=True)

    def gate_up(ch, first):
        rows, _, _ = rows_of(ch)

        def body(j, carry):
            columns = pl.ds(pl.multiple_of(256 * j, 256), 256)
            both = dot(normed[rows, :], w_gu[:, :, :, columns].reshape(2048, 256))
            hidden[rows, pl.ds(pl.multiple_of(128 * j, 128), 128)] = (
                silu(both[:, :128]) * both[:, 128:]
            ).astype(BF16)
            return carry

        if first:
            lax.fori_loop(0, 3, body, 0, unroll=True)
            return
        lax.fori_loop(3, 5, body, 0, unroll=True)
        both = dot(normed[rows, :], w_gu[:, :, :, 1280:1408].reshape(2048, 128))
        hidden[rows, 640:768] = (silu(both) * pltpu.roll(both, 64, axis=1)).astype(BF16)

    def down(ch, first):
        rows, _, _ = rows_of(ch)

        def body(p, carry):
            py, pc = lax.div(p, 2), lax.rem(p, 2)
            block = jnp.concatenate([w_d[py, 2 * pc], w_d[py, 2 * pc + 1]], axis=1)
            part2[pc, py, rows] = dot(hidden[rows, :704], block).astype(BF16)
            return carry

        lax.fori_loop(*((0, 4) if first else (4, 8)), body, 0, unroll=True)

    part = functools.partial
    actions = [part(near_own, axis=axis) for axis in range(2)]
    actions += [part(near_forward, axis=k // 2, way=k % 2) for k in range(4)]
    actions += [part(far_own, axis=k // 4, i=k % 4) for k in range(8)]
    actions += [part(far_forward, axis=k // 8, way=k // 4 % 2, i=k % 4) for k in range(16)]
    actions += [weight_done, stage_gate_up, stage_down, stage_rest]
    for tag, buf in ((10, tok), (11, resid)):
        actions.append(part(gather_own, buf, tag))
        actions += [part(gather_forward, buf, tag, side=side) for side in range(2)]
        actions += [part(gather_far, buf, tag), part(gather_done, buf, tag)]
    for tag, bufs, end in ((12, mixer_bufs, mixer_end), (13, ffn_bufs, ffn_end)):
        actions += [part(sum_pair, bufs, tag), part(sum_start, bufs, tag)]
        actions += [part(sum_relay, bufs, tag, side=side) for side in range(2)]
        actions.append(end)
    actions += [part(norm_rows, tok, mix_gain), mixer, mixer_out]
    actions += [part(norm_rows, resid, ffn_gain)]
    actions += [part(gate_up, first=True), part(gate_up, first=False)]
    actions += [part(down, first=True), part(down, first=False)]
    for code in SCHEDULE:
        actions[code // 8](code % 8)

    for name, w in enumerate((w_qo, w_gu, w_d)):
        all_sent((name, 0), w.at[0, pl.ds(0, 3)])
        all_sent((name, 1), w.at[pl.ds(0, 3)])
    for tag, buf in ((10, tok), (11, resid)):
        all_sent((tag, 0), buf.at[pl.ds(0, 3), 0])
        all_sent((tag, 1), buf.at[:, 0])
    for tag, bufs in ((12, mixer_bufs), (13, ffn_bufs)):
        all_sent((tag, 0), bufs[2].at[pl.ds(0, 3)])
        all_sent((tag, 1), bufs[0].at[0])
    for copy in stores:
        copy.wait()
    assert len(ids) == RECEIVES and len(groups) == SENDS


def per_device(*args):
    (tokens, mix_gain, query_w, key_w, value_w, gate_w, out_w, head_gain, ffn_gain) = args[:9]
    ffn_gate, ffn_up, ffn_down = args[9:]
    cosine, sine = rope_tables()
    hbm = pl.BlockSpec(memory_space=pltpu.HBM)
    rows = tokens.shape[0]

    def sum_buffers():
        return [
            pltpu.VMEM((2, 4, rows, 256), BF16),
            pltpu.VMEM((4, rows, 256), BF16),
            pltpu.VMEM((4, rows, 256), BF16),
            pltpu.VMEM((2, rows, 256), BF16),
            pltpu.VMEM((2, rows // 2, 256), BF16),
        ]

    call = pl.pallas_call(
        layer_kernel,
        out_shape=jax.ShapeDtypeStruct((rows, 256), BF16),
        in_specs=[hbm] * 15,
        out_specs=hbm,
        scratch_shapes=[
            pltpu.VMEM((4, 2, rows, 256), BF16),
            pltpu.VMEM((4, 2, rows, 256), BF16),
            pltpu.VMEM((rows, 2048), BF16),
            pltpu.VMEM((4, 4, 128, 512), BF16),
            pltpu.VMEM((4, 4, 128, 1408), BF16),
            pltpu.VMEM((4, 4, 704, 128), BF16),
            pltpu.VMEM((2 * DK, 128), BF16),
            pltpu.VMEM((1408, 128), BF16),
            pltpu.VMEM((1, 2048), F32),
            pltpu.VMEM((1, 2048), F32),
            pltpu.VMEM((1, DV), F32),
            pltpu.VMEM((SEQ, 128), F32),
            pltpu.VMEM((SEQ, 128), F32),
            pltpu.VMEM((HEADS, 8, 128), F32),
            pltpu.VMEM((rows, 256), BF16),
            pltpu.VMEM((SEQ, SEQ), F32),
            pltpu.VMEM((rows, DV), BF16),
            pltpu.VMEM((rows, 768), BF16),
            *sum_buffers(),
            *sum_buffers(),
            pltpu.SemaphoreType.DMA((32,)),
            pltpu.SemaphoreType.DMA((SENDS,)),
            pltpu.SemaphoreType.DMA((RECEIVES,)),
        ],
        compiler_params=pltpu.CompilerParams(
            collective_id=0, has_side_effects=True, vmem_limit_bytes=54 * 2**20
        ),
        cost_estimate=pl.CostEstimate(
            flops=11_000_000_000, bytes_accessed=4_000_000, transcendentals=1_000_000
        ),
        name="layer",
    )
    return call(
        tokens,
        mix_gain.reshape(1, -1),
        query_w.T,
        key_w.T,
        value_w,
        gate_w,
        out_w,
        head_gain,
        ffn_gain.reshape(1, -1),
        ffn_gate.T,
        ffn_up.T,
        ffn_down,
        jnp.asarray(cosine),
        jnp.asarray(sine),
        jnp.asarray(decay_table()),
    )


def solution(mesh):
    placed = (
        P(("rep", "fs"), "tp"),
        P(),
        P("fs", "tp"),
        P("fs", "tp"),
        P("fs", "tp"),
        P("fs", "tp"),
        P("tp", "fs"),
        P("tp", None),
        P(),
        P("fs", "tp"),
        P("fs", "tp"),
        P("tp", "fs"),
    )
    return jax.shard_map(
        per_device, mesh=mesh, in_specs=placed, out_specs=P(("rep", "fs"), "tp"), check_vma=False
    )
```

time: 102 us -> 93.7 us (0.919)
  Pallas kernels: 100 us -> 91.7 us
    pallas_call x1, Pallas kernels: 100 us -> 91.7 us  [per_device(): call(tokens, mix_gain.reshape(1, -1), query_w.T, key_w.T, value_w, gate_w...]
where the time goes in v2:
time: 93.7 us; the launch traced here: 93.6 us
  Pallas kernels  91.7 us (98%)
  local copies, waits for them, and re-layouts  1.87 us (2%)
    pallas_call x1, Pallas kernels, per_device(): call(tokens, mix_gain.reshape(1, -1), query_w.T, key_w.T, value_w, gate_w...  91.7 us

profile of v2, /device:TPU:1, one launch (start us, length us, event | category | flops | bytes accessed | tf_op | source)
XLA Modules:
  0.0 93.6 jit_solution(14810224750809273782)
XLA Ops:
  0.0 91.7 %layer.1 = bf16[1024,256]{1,0:T(8,128)(2,1)} custom-call(bf16[1024,256]{1,0:T(8,128)(2,1)} %tok_hbm.1, f32[1,2048]{1,0:T(1,128)} %bitcast.10, bf16[64,128]{1,0:T(8,128)(2,1)} %bitcast.8, bf16[64,128]{1,0:T(8,128)(2,1)} %bitcast.9, bf16[128,128]{1,0:T(8,128)(2,1)} %value_hbm.1, bf16[128,128]{1,0:T(8,128)(2,1)} %gate_hbm.1, bf16[128,128]{1,0:T(8,128)(2,1)} %out_w_hbm.1, ...), custom_call_target="tpu_custom_call" | custom-call | flops 11000000512 | bytes 4000000 | tf_op jit(solution)/shard_map/layer/pallas_call | solution.py:561
  91.7 1.9 %copy.17 = bf16[1024,256]{1,0:T(8,128)(2,1)} copy(bf16[1024,256]{1,0:T(8,128)(2,1)} %layer.1) | data formatting | bytes 1048576

commit v3 on v2

--- a/solution.py
+++ b/solution.py
@@ -17,36 +17,38 @@
 F32 = jnp.float32
 BF16 = jnp.bfloat16
 MESH = pl.DeviceIdType.MESH
-RECEIVES = 179
-SENDS = 14
+RECEIVES = 195
+SENDS = 18
 
 UNITS = (
     (0, 64, 32, 64, 32),
     (0, 32, 16, 32, 16),
     (64, 32, 16, 32, 16),
     (0, 176, 96, 176, 96),
-    (352, 176, 96, 176, 96),
+    (0, 176, 96, 176, 96),
 )
-WEIGHT_OF = (0, 1, 1, 2, 2)
+WEIGHT_OF = (0, 1, 1, 2, 3)
 
 SCHEDULE = (
-    8, 0, 274, 48, 248, 275, 80, 10, 2, 272, 40, 32, 24, 16, 64, 96,
-    282, 290, 144, 112, 176, 56, 208, 256, 88, 104, 72, 291, 9, 1, 283, 280,
-    288, 273, 264, 192, 216, 120, 128, 184, 160, 224, 152, 298, 200, 232, 168, 136,
-    82, 299, 4, 50, 26, 42, 34, 66, 306, 434, 18, 12, 33, 90, 307, 11,
-    296, 435, 25, 41, 98, 58, 240, 443, 451, 355, 281, 304, 17, 289, 442, 106,
-    450, 354, 363, 81, 74, 432, 210, 440, 297, 44, 362, 36, 448, 194, 130, 146,
-    52, 352, 162, 305, 154, 114, 122, 3, 178, 35, 371, 379, 226, 218, 360, 43,
-    202, 186, 433, 170, 138, 234, 378, 370, 20, 97, 57, 51, 441, 387, 65, 105,
-    315, 449, 376, 19, 27, 353, 49, 28, 83, 242, 368, 89, 59, 386, 99, 68,
-    314, 361, 108, 67, 323, 73, 107, 91, 75, 100, 384, 115, 153, 92, 217, 331,
-    193, 76, 113, 60, 201, 233, 121, 225, 148, 322, 330, 377, 369, 84, 137, 161,
-    169, 185, 312, 145, 177, 339, 236, 209, 228, 211, 171, 147, 187, 204, 129, 163,
-    123, 227, 139, 219, 131, 155, 338, 195, 347, 179, 235, 220, 203, 164, 116, 132,
-    385, 313, 346, 196, 124, 156, 172, 188, 180, 140, 459, 212, 458, 241, 320, 328,
-    467, 466, 243, 475, 244, 483, 329, 321, 491, 395, 474, 336, 482, 490, 394, 403,
-    344, 456, 464, 337, 402, 472, 480, 488, 392, 345, 457, 419, 411, 465, 400, 473,
-    481, 489, 393, 418, 410, 427, 401, 408, 416, 426, 417, 409, 424, 425,
+    0, 8, 273, 80, 48, 248, 272, 256, 274, 1, 9, 24, 16, 40, 32, 96,
+    56, 88, 289, 281, 264, 64, 11, 3, 288, 280, 72, 104, 275, 2, 10, 160,
+    290, 208, 192, 112, 176, 144, 184, 216, 224, 152, 297, 120, 282, 128, 296, 168,
+    136, 200, 232, 305, 12, 27, 35, 67, 19, 33, 4, 43, 51, 91, 473, 59,
+    304, 49, 18, 41, 25, 472, 99, 283, 17, 83, 291, 65, 97, 26, 50, 89,
+    240, 480, 488, 352, 298, 481, 489, 299, 353, 360, 306, 107, 474, 482, 307, 81,
+    75, 361, 490, 147, 42, 57, 82, 195, 354, 115, 34, 475, 483, 376, 368, 491,
+    179, 235, 155, 123, 211, 203, 362, 163, 139, 355, 171, 227, 131, 187, 219, 66,
+    105, 44, 377, 73, 58, 369, 98, 90, 113, 129, 384, 312, 106, 243, 74, 209,
+    378, 177, 217, 185, 161, 121, 370, 363, 385, 145, 201, 153, 137, 225, 193, 36,
+    169, 178, 536, 328, 320, 130, 114, 20, 146, 313, 233, 386, 154, 186, 28, 210,
+    202, 379, 194, 234, 371, 218, 122, 226, 138, 170, 162, 84, 314, 60, 336, 241,
+    344, 76, 92, 68, 496, 52, 100, 321, 108, 329, 387, 315, 242, 504, 512, 322,
+    212, 188, 180, 330, 140, 164, 124, 337, 228, 220, 172, 156, 196, 132, 520, 116,
+    204, 236, 148, 392, 345, 497, 505, 323, 331, 400, 513, 338, 521, 393, 244, 537,
+    528, 346, 432, 529, 433, 401, 498, 506, 339, 440, 514, 522, 394, 416, 408, 347,
+    441, 530, 434, 499, 409, 417, 402, 507, 442, 515, 523, 395, 424, 448, 456, 531,
+    435, 457, 449, 425, 403, 443, 418, 410, 450, 458, 464, 465, 411, 419, 459, 451,
+    426, 466, 427, 467,
 )
 
 
@@ -92,13 +94,16 @@
     cos_hbm,
     sin_hbm,
     rate_hbm,
-    out_hbm,
+    out_ref,
     tok,
     resid,
     normed,
     w_qo,
     w_gu,
-    w_d,
+    w_d0,
+    w_d1,
+    joined,
+    down_in,
     turn_qk,
     turn_gu,
     mix_gain,
@@ -107,7 +112,6 @@
     cos_ref,
     sin_ref,
     rate_ref,
-    out_ref,
     mask,
     mixed,
     hidden,
@@ -121,6 +125,12 @@
     sums2,
     ends2,
     relay2,
+    part3,
+    pair3,
+    sums3,
+    ends3,
+    relay3,
+    first,
     local_sem,
     send_sem,
     recv_sem,
@@ -210,7 +220,7 @@
         for k, source in enumerate((ffn_gate_hbm, ffn_up_hbm)):
             place = pl.ds(256 * j + width * k, width)
             load_gu.append(local(source.at[pl.ds(128 * j, width)], turn_gu.at[place]))
-    load_down = [local(down_hbm, w_d.at[z, x])]
+    load_down = [local(down_hbm, down_in)]
     load_rest = [
         local(mix_gain_hbm, mix_gain),
         local(ffn_gain_hbm, ffn_gain),
@@ -238,6 +248,9 @@
 
     def stage_down(_):
         loaded(load_down)
+        top, low = down_in[0:352, :], down_in[352:704, :]
+        w_d0[z, x] = jnp.concatenate([top[:, :64], low[:, :64]], axis=1)
+        w_d1[z, x] = jnp.concatenate([top[:, 64:], low[:, 64:]], axis=1)
 
     def stage_rest(_):
         loaded(load_rest)
@@ -277,7 +290,7 @@
         rows, _, _ = rows_of(ch)
         recv((tag, 3, ch), buf.at[:, oc, rows])
 
-    buffers = (w_qo, w_gu, w_gu, w_d, w_d)
+    buffers = (w_qo, w_gu, w_gu, w_d0, w_d1)
 
     def spans(unit):
         first, a, a0, b, b0 = UNITS[unit]
@@ -334,7 +347,10 @@
         recv((unit, 3), buffers[unit].at[0, :, pl.ds(first, a + b)])
 
     mixer_bufs = (part1, pair1, sums1, ends1, relay1)
-    ffn_bufs = (part2, pair2, sums2, ends2, relay2)
+    ffn_bufs = (
+        (part2, pair2, sums2, ends2, relay2),
+        (part3, pair3, sums3, ends3, relay3),
+    )
 
     def sum_pair(bufs, tag, ch):
         part, pair = bufs[:2]
@@ -381,27 +397,33 @@
         total = sum_end(mixer_bufs, 12, ch)
         resid[y, c, rows] = (tok[y, c, rows].astype(F32) + total).astype(BF16)
 
-    def ffn_end(ch):
-        rows, _, _ = rows_of(ch)
-        total = sum_end(ffn_bufs, 13, ch)
+    def ffn_end(ch, half):
+        rows, _, _ = rows_of(ch)
+        total = sum_end(ffn_bufs[half], 13 + half, ch)
+        if half == 0:
+            first[rows] = total
+            return
+        total = jnp.concatenate(
+            [first[rows, :64], total[:, :64], first[rows, 64:], total[:, 64:]], axis=1
+        )
         out_ref[rows, :] = (resid[y, c, rows].astype(F32) + total).astype(BF16)
-        stores.append(local(out_ref.at[rows], out_hbm.at[rows]))
 
     def norm_rows(buf, gain, ch):
         def body(i, carry):
             rows = pl.ds(pl.multiple_of(SEQ * ch + 32 * i, 32), 32)
-            blocks = [buf[p // 2, p % 2, rows].astype(F32) for p in range(8)]
-            squares = blocks[0] * blocks[0]
-            for block in blocks[1:]:
-                squares = squares + block * block
+            squares = None
+            for p in range(8):
+                block = buf[p // 2, p % 2, rows].astype(F32)
+                squares = block * block if p == 0 else squares + block * block
             mean = jnp.sum(squares, axis=-1, keepdims=True) * (1.0 / 2048.0)
             factor = lax.rsqrt(mean + EPS)
             for p in range(8):
                 lanes = slice(256 * p, 256 * p + 256)
-                normed[rows, lanes] = (blocks[p] * factor * gain[:, lanes]).astype(BF16)
+                block = buf[p // 2, p % 2, rows].astype(F32)
+                normed[rows, lanes] = (block * factor * gain[:, lanes]).astype(BF16)
             return carry
 
-        lax.fori_loop(0, 8, body, 0)
+        lax.fori_loop(0, 8, body, 0, unroll=4)
 
     def mixer(ch):
         rows, _, _ = rows_of(ch)
@@ -458,16 +480,24 @@
         both = dot(normed[rows, :], w_gu[:, :, :, 1280:1408].reshape(2048, 128))
         hidden[rows, 640:768] = (silu(both) * pltpu.roll(both, 64, axis=1)).astype(BF16)
 
-    def down(ch, first):
-        rows, _, _ = rows_of(ch)
-
-        def body(p, carry):
-            py, pc = lax.div(p, 2), lax.rem(p, 2)
-            block = jnp.concatenate([w_d[py, 2 * pc], w_d[py, 2 * pc + 1]], axis=1)
-            part2[pc, py, rows] = dot(hidden[rows, :704], block).astype(BF16)
-            return carry
-
-        lax.fori_loop(*((0, 4) if first else (4, 8)), body, 0, unroll=True)
+    def join(half):
+        w = (w_d0, w_d1)[half]
+        for py in range(4):
+            top, low = [], []
+            for k in range(4):
+                block = w[py, k]
+                top.append(block[:, :64])
+                low.append(block[:, 64:])
+            joined[half, py, 0:352, :] = jnp.concatenate(top, axis=1)
+            joined[half, py, 352:704, :] = jnp.concatenate(low, axis=1)
+
+    def down(ch, half):
+        rows, _, _ = rows_of(ch)
+        target = (part2, part3)[half]
+        for py in range(4):
+            both = dot(hidden[rows, :704], joined[half, py]).astype(BF16)
+            target[0, py, rows] = both[:, :128]
+            target[1, py, rows] = both[:, 128:]
 
     part = functools.partial
     actions = [part(near_own, axis=axis) for axis in range(2)]
@@ -479,24 +509,28 @@
         actions.append(part(gather_own, buf, tag))
         actions += [part(gather_forward, buf, tag, side=side) for side in range(2)]
         actions += [part(gather_far, buf, tag), part(gather_done, buf, tag)]
-    for tag, bufs, end in ((12, mixer_bufs, mixer_end), (13, ffn_bufs, ffn_end)):
+    for tag, bufs, end in (
+        (12, mixer_bufs, mixer_end),
+        (13, ffn_bufs[0], part(ffn_end, half=0)),
+        (14, ffn_bufs[1], part(ffn_end, half=1)),
+    ):
         actions += [part(sum_pair, bufs, tag), part(sum_start, bufs, tag)]
         actions += [part(sum_relay, bufs, tag, side=side) for side in range(2)]
         actions.append(end)
     actions += [part(norm_rows, tok, mix_gain), mixer, mixer_out]
     actions += [part(norm_rows, resid, ffn_gain)]
     actions += [part(gate_up, first=True), part(gate_up, first=False)]
-    actions += [part(down, first=True), part(down, first=False)]
+    actions += [part(down, half=0), part(down, half=1), join]
     for code in SCHEDULE:
         actions[code // 8](code % 8)
 
-    for name, w in enumerate((w_qo, w_gu, w_d)):
+    for name, w in enumerate((w_qo, w_gu, w_d0, w_d1)):
         all_sent((name, 0), w.at[0, pl.ds(0, 3)])
         all_sent((name, 1), w.at[pl.ds(0, 3)])
     for tag, buf in ((10, tok), (11, resid)):
         all_sent((tag, 0), buf.at[pl.ds(0, 3), 0])
         all_sent((tag, 1), buf.at[:, 0])
-    for tag, bufs in ((12, mixer_bufs), (13, ffn_bufs)):
+    for tag, bufs in ((12, mixer_bufs), (13, ffn_bufs[0]), (14, ffn_bufs[1])):
         all_sent((tag, 0), bufs[2].at[pl.ds(0, 3)])
         all_sent((tag, 1), bufs[0].at[0])
     for copy in stores:
@@ -511,27 +545,30 @@
     hbm = pl.BlockSpec(memory_space=pltpu.HBM)
     rows = tokens.shape[0]
 
-    def sum_buffers():
+    def sum_buffers(width):
         return [
-            pltpu.VMEM((2, 4, rows, 256), BF16),
-            pltpu.VMEM((4, rows, 256), BF16),
-            pltpu.VMEM((4, rows, 256), BF16),
-            pltpu.VMEM((2, rows, 256), BF16),
-            pltpu.VMEM((2, rows // 2, 256), BF16),
+            pltpu.VMEM((2, 4, rows, width), BF16),
+            pltpu.VMEM((4, rows, width), BF16),
+            pltpu.VMEM((4, rows, width), BF16),
+            pltpu.VMEM((2, rows, width), BF16),
+            pltpu.VMEM((2, rows // 2, width), BF16),
         ]
 
     call = pl.pallas_call(
         layer_kernel,
-        out_shape=jax.ShapeDtypeStruct((rows, 256), BF16),
+        out_shape=pltpu.VMEM((rows, 256), BF16),
         in_specs=[hbm] * 15,
-        out_specs=hbm,
+        out_specs=pl.BlockSpec(memory_space=pltpu.VMEM),
         scratch_shapes=[
             pltpu.VMEM((4, 2, rows, 256), BF16),
             pltpu.VMEM((4, 2, rows, 256), BF16),
             pltpu.VMEM((rows, 2048), BF16),
             pltpu.VMEM((4, 4, 128, 512), BF16),
             pltpu.VMEM((4, 4, 128, 1408), BF16),
-            pltpu.VMEM((4, 4, 704, 128), BF16),
+            pltpu.VMEM((4, 4, 352, 128), BF16),
+            pltpu.VMEM((4, 4, 352, 128), BF16),
+            pltpu.VMEM((2, 4, 704, 256), BF16),
+            pltpu.VMEM((704, 128), BF16),
             pltpu.VMEM((2 * DK, 128), BF16),
             pltpu.VMEM((1408, 128), BF16),
             pltpu.VMEM((1, 2048), F32),
@@ -540,12 +577,13 @@
             pltpu.VMEM((SEQ, 128), F32),
             pltpu.VMEM((SEQ, 128), F32),
             pltpu.VMEM((HEADS, 8, 128), F32),
-            pltpu.VMEM((rows, 256), BF16),
             pltpu.VMEM((SEQ, SEQ), F32),
             pltpu.VMEM((rows, DV), BF16),
             pltpu.VMEM((rows, 768), BF16),
-            *sum_buffers(),
-            *sum_buffers(),
+            *sum_buffers(256),
+            *sum_buffers(128),
+            *sum_buffers(128),
+            pltpu.VMEM((rows, 128), F32),
             pltpu.SemaphoreType.DMA((32,)),
             pltpu.SemaphoreType.DMA((SENDS,)),
             pltpu.SemaphoreType.DMA((RECEIVES,)),

time: 93.7 us -> 91.4 us (0.975)
  Pallas kernels: 91.7 us -> 90.4 us
  local copies, waits for them, and re-layouts: 1.87 us -> 0.8 us
    pallas_call x1, Pallas kernels: 91.7 us -> 90.4 us  [per_device(): call(tokens, mix_gain.reshape(1, -1), query_w.T, key_w.T, value_w, gate_w...]
    unnamed x1, local copies, waits for them, and re-layouts: 1.87 us -> 0.8 us
where the time goes in v3:
time: 91.4 us; the launch traced here: 91.2 us
  Pallas kernels  90.4 us (99%)
    pallas_call x1, Pallas kernels, per_device(): call(tokens, mix_gain.reshape(1, -1), query_w.T, key_w.T, value_w, gate_w...  90.4 us

profile of v3, /device:TPU:1, one launch (start us, length us, event | category | flops | bytes accessed | tf_op | source)
XLA Modules:
  0.0 91.2 jit_solution(5749314618804656369)
XLA Ops:
  0.0 90.4 %layer.1 = bf16[1024,256]{1,0:T(8,128)(2,1)S(1)} custom-call(bf16[1024,256]{1,0:T(8,128)(2,1)} %tok_hbm.1, f32[1,2048]{1,0:T(1,128)} %bitcast.10, bf16[64,128]{1,0:T(8,128)(2,1)} %bitcast.8, bf16[64,128]{1,0:T(8,128)(2,1)} %bitcast.9, bf16[128,128]{1,0:T(8,128)(2,1)} %value_hbm.1, bf16[128,128]{1,0:T(8,128)(2,1)} %gate_hbm.1, bf16[128,128]{1,0:T(8,128)(2,1)} %out_w_hbm.1, ...), custom_call_target="tpu_custom_call" | custom-call | flops 11000000512 | bytes 4000000 | tf_op jit(solution)/shard_map/layer/pallas_call | solution.py:599
  90.4 0.8 copy.17

commit v4 on v3

--- a/solution.py
+++ b/solution.py
@@ -30,25 +30,25 @@
 WEIGHT_OF = (0, 1, 1, 2, 3)
 
 SCHEDULE = (
-    0, 8, 273, 80, 48, 248, 272, 256, 274, 1, 9, 24, 16, 40, 32, 96,
-    56, 88, 289, 281, 264, 64, 11, 3, 288, 280, 72, 104, 275, 2, 10, 160,
-    290, 208, 192, 112, 176, 144, 184, 216, 224, 152, 297, 120, 282, 128, 296, 168,
-    136, 200, 232, 305, 12, 27, 35, 67, 19, 33, 4, 43, 51, 91, 473, 59,
-    304, 49, 18, 41, 25, 472, 99, 283, 17, 83, 291, 65, 97, 26, 50, 89,
-    240, 480, 488, 352, 298, 481, 489, 299, 353, 360, 306, 107, 474, 482, 307, 81,
-    75, 361, 490, 147, 42, 57, 82, 195, 354, 115, 34, 475, 483, 376, 368, 491,
-    179, 235, 155, 123, 211, 203, 362, 163, 139, 355, 171, 227, 131, 187, 219, 66,
-    105, 44, 377, 73, 58, 369, 98, 90, 113, 129, 384, 312, 106, 243, 74, 209,
-    378, 177, 217, 185, 161, 121, 370, 363, 385, 145, 201, 153, 137, 225, 193, 36,
-    169, 178, 536, 328, 320, 130, 114, 20, 146, 313, 233, 386, 154, 186, 28, 210,
-    202, 379, 194, 234, 371, 218, 122, 226, 138, 170, 162, 84, 314, 60, 336, 241,
-    344, 76, 92, 68, 496, 52, 100, 321, 108, 329, 387, 315, 242, 504, 512, 322,
-    212, 188, 180, 330, 140, 164, 124, 337, 228, 220, 172, 156, 196, 132, 520, 116,
-    204, 236, 148, 392, 345, 497, 505, 323, 331, 400, 513, 338, 521, 393, 244, 537,
-    528, 346, 432, 529, 433, 401, 498, 506, 339, 440, 514, 522, 394, 416, 408, 347,
-    441, 530, 434, 499, 409, 417, 402, 507, 442, 515, 523, 395, 424, 448, 456, 531,
-    435, 457, 449, 425, 403, 443, 418, 410, 450, 458, 464, 465, 411, 419, 459, 451,
-    426, 466, 427, 467,
+    0, 8, 274, 272, 80, 248, 48, 9, 2, 16, 24, 40, 32, 273, 96, 264,
+    64, 56, 144, 176, 208, 282, 88, 290, 112, 288, 72, 104, 1, 280, 275, 10,
+    128, 289, 160, 192, 120, 184, 224, 216, 256, 298, 152, 168, 136, 232, 200, 11,
+    296, 81, 306, 281, 49, 33, 474, 41, 17, 25, 97, 57, 304, 65, 3, 472,
+    89, 283, 291, 240, 480, 488, 352, 297, 482, 490, 299, 105, 73, 177, 354, 360,
+    305, 473, 481, 307, 225, 121, 145, 489, 362, 209, 153, 113, 185, 217, 129, 193,
+    161, 353, 475, 483, 233, 169, 137, 201, 376, 368, 491, 34, 12, 35, 42, 19,
+    26, 361, 4, 18, 27, 370, 378, 43, 52, 82, 51, 241, 83, 59, 384, 312,
+    50, 98, 99, 106, 377, 74, 355, 58, 90, 369, 210, 36, 44, 386, 66, 314,
+    67, 91, 20, 363, 75, 328, 28, 100, 385, 320, 107, 170, 138, 154, 178, 322,
+    218, 122, 146, 202, 226, 330, 194, 114, 162, 379, 371, 313, 130, 186, 234, 147,
+    84, 60, 92, 123, 68, 76, 219, 108, 187, 336, 195, 115, 179, 171, 163, 148,
+    211, 203, 139, 196, 338, 235, 344, 228, 155, 131, 116, 227, 496, 387, 315, 242,
+    346, 498, 506, 156, 124, 220, 180, 504, 321, 329, 188, 132, 212, 204, 236, 172,
+    164, 140, 514, 512, 243, 536, 522, 394, 331, 323, 520, 392, 244, 337, 537, 402,
+    530, 434, 528, 400, 345, 432, 497, 505, 339, 442, 513, 440, 521, 418, 393, 410,
+    347, 529, 499, 416, 408, 507, 401, 433, 515, 450, 458, 523, 395, 456, 448, 531,
+    435, 441, 426, 424, 403, 443, 466, 409, 417, 464, 457, 449, 411, 419, 451, 459,
+    425, 465, 427, 467,
 )
 
 
@@ -390,8 +390,6 @@
             ends[0, rows].astype(F32) + ends[1, rows].astype(F32)
         )
 
-    stores = []
-
     def mixer_end(ch):
         rows, _, _ = rows_of(ch)
         total = sum_end(mixer_bufs, 12, ch)
@@ -533,8 +531,6 @@
     for tag, bufs in ((12, mixer_bufs), (13, ffn_bufs[0]), (14, ffn_bufs[1])):
         all_sent((tag, 0), bufs[2].at[pl.ds(0, 3)])
         all_sent((tag, 1), bufs[0].at[0])
-    for copy in stores:
-        copy.wait()
     assert len(ids) == RECEIVES and len(groups) == SENDS
 
 

time: 91.4 us -> 90.3 us (0.988)
  Pallas kernels: 90.4 us -> 89.3 us
    pallas_call x1, Pallas kernels: 90.4 us -> 89.3 us  [per_device(): call(tokens, mix_gain.reshape(1, -1), query_w.T, key_w.T, value_w, gate_w...]
where the time goes in v4:
time: 90.3 us; the launch traced here: 90.1 us
  Pallas kernels  89.3 us (99%)
    pallas_call x1, Pallas kernels, per_device(): call(tokens, mix_gain.reshape(1, -1), query_w.T, key_w.T, value_w, gate_w...  89.3 us

profile of v4, /device:TPU:1, one launch (start us, length us, event | category | flops | bytes accessed | tf_op | source)
XLA Modules:
  0.0 90.1 jit_solution(11593004546300200195)
XLA Ops:
  0.0 89.3 %layer.1 = bf16[1024,256]{1,0:T(8,128)(2,1)S(1)} custom-call(bf16[1024,256]{1,0:T(8,128)(2,1)} %tok_hbm.1, f32[1,2048]{1,0:T(1,128)} %bitcast.10, bf16[64,128]{1,0:T(8,128)(2,1)} %bitcast.8, bf16[64,128]{1,0:T(8,128)(2,1)} %bitcast.9, bf16[128,128]{1,0:T(8,128)(2,1)} %value_hbm.1, bf16[128,128]{1,0:T(8,128)(2,1)} %gate_hbm.1, bf16[128,128]{1,0:T(8,128)(2,1)} %out_w_hbm.1, ...), custom_call_target="tpu_custom_call" | custom-call | flops 11000000512 | bytes 4000000 | tf_op jit(solution)/shard_map/layer/pallas_call | solution.py:595
  89.3 0.8 copy.17

commit v5 on v4

--- a/solution.py
+++ b/solution.py
@@ -30,25 +30,25 @@
 WEIGHT_OF = (0, 1, 1, 2, 3)
 
 SCHEDULE = (
-    0, 8, 274, 272, 80, 248, 48, 9, 2, 16, 24, 40, 32, 273, 96, 264,
-    64, 56, 144, 176, 208, 282, 88, 290, 112, 288, 72, 104, 1, 280, 275, 10,
-    128, 289, 160, 192, 120, 184, 224, 216, 256, 298, 152, 168, 136, 232, 200, 11,
-    296, 81, 306, 281, 49, 33, 474, 41, 17, 25, 97, 57, 304, 65, 3, 472,
-    89, 283, 291, 240, 480, 488, 352, 297, 482, 490, 299, 105, 73, 177, 354, 360,
-    305, 473, 481, 307, 225, 121, 145, 489, 362, 209, 153, 113, 185, 217, 129, 193,
-    161, 353, 475, 483, 233, 169, 137, 201, 376, 368, 491, 34, 12, 35, 42, 19,
-    26, 361, 4, 18, 27, 370, 378, 43, 52, 82, 51, 241, 83, 59, 384, 312,
-    50, 98, 99, 106, 377, 74, 355, 58, 90, 369, 210, 36, 44, 386, 66, 314,
-    67, 91, 20, 363, 75, 328, 28, 100, 385, 320, 107, 170, 138, 154, 178, 322,
-    218, 122, 146, 202, 226, 330, 194, 114, 162, 379, 371, 313, 130, 186, 234, 147,
-    84, 60, 92, 123, 68, 76, 219, 108, 187, 336, 195, 115, 179, 171, 163, 148,
-    211, 203, 139, 196, 338, 235, 344, 228, 155, 131, 116, 227, 496, 387, 315, 242,
-    346, 498, 506, 156, 124, 220, 180, 504, 321, 329, 188, 132, 212, 204, 236, 172,
-    164, 140, 514, 512, 243, 536, 522, 394, 331, 323, 520, 392, 244, 337, 537, 402,
-    530, 434, 528, 400, 345, 432, 497, 505, 339, 442, 513, 440, 521, 418, 393, 410,
-    347, 529, 499, 416, 408, 507, 401, 433, 515, 450, 458, 523, 395, 456, 448, 531,
-    435, 441, 426, 424, 403, 443, 466, 409, 417, 464, 457, 449, 411, 419, 451, 459,
-    425, 465, 427, 467,
+    0, 8, 273, 272, 80, 264, 48, 248, 9, 1, 16, 24, 32, 40, 64, 88,
+    289, 281, 56, 96, 275, 208, 176, 72, 104, 280, 144, 288, 112, 33, 184, 128,
+    2, 41, 160, 216, 297, 274, 152, 305, 224, 120, 192, 168, 136, 200, 232, 49,
+    25, 296, 291, 283, 256, 65, 105, 10, 17, 89, 97, 473, 57, 81, 304, 3,
+    472, 282, 290, 240, 480, 488, 352, 299, 481, 489, 73, 201, 353, 360, 307, 298,
+    475, 113, 161, 11, 145, 233, 129, 185, 483, 225, 306, 361, 491, 121, 153, 355,
+    193, 217, 474, 209, 177, 137, 169, 50, 82, 368, 376, 482, 363, 490, 18, 34,
+    27, 369, 42, 43, 19, 4, 59, 354, 90, 67, 12, 241, 26, 377, 384, 312,
+    58, 98, 371, 35, 28, 106, 66, 99, 75, 379, 385, 313, 74, 178, 362, 20,
+    107, 44, 91, 83, 218, 51, 36, 122, 84, 328, 320, 387, 60, 194, 210, 162,
+    146, 321, 329, 202, 154, 130, 138, 226, 378, 234, 370, 186, 114, 170, 108, 92,
+    211, 315, 195, 76, 68, 100, 52, 163, 115, 147, 336, 227, 179, 131, 219, 139,
+    212, 187, 123, 156, 171, 203, 180, 337, 155, 344, 496, 235, 124, 386, 314, 242,
+    345, 504, 140, 204, 497, 164, 220, 505, 323, 331, 132, 148, 188, 116, 236, 228,
+    196, 172, 513, 512, 243, 536, 520, 392, 322, 330, 521, 393, 244, 339, 537, 400,
+    529, 433, 528, 432, 347, 401, 499, 507, 338, 441, 515, 440, 523, 408, 395, 346,
+    531, 498, 416, 409, 417, 506, 403, 435, 514, 457, 449, 522, 394, 456, 448, 443,
+    530, 434, 424, 425, 402, 442, 465, 411, 464, 419, 451, 459, 410, 418, 450, 458,
+    427, 467, 426, 466,
 )
 
 

time: 90.3 us -> 90.5 us (level)
  no operation moved by 1% of the time
where the time goes in v5:
time: 90.5 us; the launch traced here: 90.4 us
  Pallas kernels  89.6 us (99%)
    pallas_call x1, Pallas kernels, per_device(): call(tokens, mix_gain.reshape(1, -1), query_w.T, key_w.T, value_w, gate_w...  89.6 us

profile of v5, /device:TPU:1, one launch (start us, length us, event | category | flops | bytes accessed | tf_op | source)
XLA Modules:
  0.0 90.4 jit_solution(17967693817553265837)
XLA Ops:
  0.0 89.6 %layer.1 = bf16[1024,256]{1,0:T(8,128)(2,1)S(1)} custom-call(bf16[1024,256]{1,0:T(8,128)(2,1)} %tok_hbm.1, f32[1,2048]{1,0:T(1,128)} %bitcast.10, bf16[64,128]{1,0:T(8,128)(2,1)} %bitcast.8, bf16[64,128]{1,0:T(8,128)(2,1)} %bitcast.9, bf16[128,128]{1,0:T(8,128)(2,1)} %value_hbm.1, bf16[128,128]{1,0:T(8,128)(2,1)} %gate_hbm.1, bf16[128,128]{1,0:T(8,128)(2,1)} %out_w_hbm.1, ...), custom_call_target="tpu_custom_call" | custom-call | flops 11000000512 | bytes 4000000 | tf_op jit(solution)/shard_map/layer/pallas_call | solution.py:595
  89.6 0.8 copy.17
